TPU v7x, 32 devices: a whole 2x2x4 slice. The times are simulated.
32 devices in a mesh: ep: 32 (over z, y, x, core).
Axes of the slice: x: 2, y: 2, z: 4, core: 2. Of those that a mesh axis runs over, the one named last changes fastest.
Arguments:
- tokens: bfloat16 [768, 2048], P('ep'), may hold values from -6 to 6
- state: float32 [768, 16, 64, 64], P('ep'), may hold values from -4 to 4
- norm_gain: float32 [2048], replicated, may hold values from 0.1 to 1.9
- w_recept: bfloat16 [2048, 1024], replicated, may hold values from -0.125 to 0.125
- w_keys: bfloat16 [2048, 1024], replicated, may hold values from -0.125 to 0.125
- w_values: bfloat16 [2048, 1024], replicated, may hold values from -0.125 to 0.125
- decay_base: float32 [1024], replicated, may hold values from -3 to 3
- decay_first_matrix: bfloat16 [2048, 128], replicated, may hold values from -0.125 to 0.125
- decay_second_matrix: bfloat16 [128, 1024], replicated, may hold values from -0.5 to 0.5
- rate_base: float32 [1024], replicated, may hold values from -3 to 3
- rate_first_matrix: bfloat16 [2048, 128], replicated, may hold values from -0.125 to 0.125
- rate_second_matrix: bfloat16 [128, 1024], replicated, may hold values from -0.5 to 0.5
- head_gain: float32 [1024], replicated, may hold values from 0.1 to 1.9
- w_output: bfloat16 [1024, 2048], replicated, may hold values from -0.1875 to 0.1875
- second_gain: float32 [2048], replicated, may hold values from 0.1 to 1.9
- route_ids: int32 [768, 2], replicated, may hold values from 0 to 15, all different within a row; in each aligned block of 24 rows (0 to 23, 24 to 47, ...) at most 6 rows name the same one
- route_weights: float32 [768, 2], replicated, may hold values from 0.2 to 1
- expert_gate: bfloat16 [2048, 49152], P(None, 'ep'), may hold values from -0.125 to 0.125
- expert_up: bfloat16 [2048, 49152], P(None, 'ep'), may hold values from -0.125 to 0.125
- expert_down: bfloat16 [49152, 2048], P('ep'), may hold values from -0.109375 to 0.109375
Outputs:
- layer_out: bfloat16 [768, 2048], P('ep')
- new_state: float32 [768, 16, 64, 64], P('ep')
Inputs may be any that keep to these rules, and one draw needn't show every extreme that they name: `route_ids`: each row names 2 different experts. Among the 24 rows of one device (aligned blocks), no expert is named by more than 6 rows, and in every draw some block names some expert exactly 6 times.
All inputs are finite; a program needn't handle non-finite values.
Results may differ from a plain program's by a relative error of at most 0.015.
Values may be sent and summed in bfloat16 or wider, within the bound.
A program may use at most 192 MiB of HBM per device.

v0:
```python
import functools
import math

import jax
import jax.numpy as jnp
import numpy as np
from jax import lax
from jax.experimental import pallas as pl
from jax.experimental.pallas import tpu as pltpu
from jax.sharding import PartitionSpec as P

EXPERTS = 16
CAP_DEV = 6
ROWS = 8
PARTS = 3
MESH = pl.DeviceIdType.MESH
BF = jnp.bfloat16
F32 = jnp.float32


def dot(a, b):
    return jnp.dot(a, b, preferred_element_type=F32)


def mixer_kernel(
    tokens, norm_gain, decay_base, rate_base, head_gain, second_gain, order, share,
    state, w_recept, w_keys, w_values, d_first, d_second, r_first, r_second, w_output,
    new_state, after_ref, packed_ref, blend_ref,
    st, wr, wk, wv, df, ds, rf, rs, wo, kh, dh, ah, vt, rt, mt,
    w_sem, in_sem, out_sem,
):
    count, heads, width, _ = state.shape
    loads = [
        pltpu.make_async_copy(src, dst, w_sem.at[i])
        for i, (src, dst) in enumerate(
            [
                (d_first, df), (r_first, rf), (w_keys, wk), (w_values, wv), (d_second, ds),
                (r_second, rs), (w_recept, wr), (w_output, wo),
            ]
        )
    ]
    for copy in loads[:7]:
        copy.start()

    def fetch(h):
        return pltpu.make_async_copy(state.at[:, h], st.at[h], in_sem.at[h])

    def put(h):
        return pltpu.make_async_copy(st.at[h], new_state.at[:, h], out_sem.at[h])

    def start_fetch(h, c):
        fetch(h).start()
        return c

    def start_fetches(turn_at):
        low, high = turn_at * heads // 3, (turn_at + 1) * heads // 3
        lax.fori_loop(low, high, start_fetch, 0)

    shape = (EXPERTS, ROWS, count)
    slot = jnp.broadcast_to(order[...][:, None, :], shape)
    weight = jnp.broadcast_to(share[...][:, None, :], shape)
    at = lax.broadcasted_iota(jnp.int32, shape, 1)
    table = []
    for j in range(PARTS + 1):
        if j == PARTS:
            hits = (slot == at) & (at < CAP_DEV)
        else:
            hits = (slot == (at - CAP_DEV) * PARTS + j) & (at >= CAP_DEV)
        hits = jnp.where(hits, 1.0, 0.0)
        blend_ref[j] = (hits * weight).reshape(EXPERTS * ROWS, count)
        table.append(hits.reshape(EXPERTS * ROWS, count).astype(BF))

    resid = tokens[...].astype(F32)
    mean_sq = jnp.mean(resid * resid, axis=-1, keepdims=True)
    normed = (resid * lax.rsqrt(mean_sq + 1e-06) * norm_gain[...]).astype(BF)

    def spread(ref, values):
        for h in range(heads):
            ref[h] = values[:, h * width:(h + 1) * width]

    lanes = vt.shape[1]

    def turn(values):
        blank = jnp.zeros((lanes - count, values.shape[1]), F32)
        return jnp.concatenate([values, blank], axis=0).T

    loads[0].wait()
    decay_low = jnp.tanh(dot(normed, df[...])).astype(BF)
    loads[1].wait()
    rate_low = dot(normed, rf[...]).astype(BF)
    loads[2].wait()
    spread(kh, dot(normed, wk[...]).astype(BF).astype(F32))
    start_fetches(0)
    loads[3].wait()
    vals = dot(normed, wv[...]).astype(BF).astype(F32)
    vt[...] = turn(vals)
    start_fetches(1)
    loads[4].wait()
    pre = decay_base[...] + dot(decay_low, ds[...])
    spread(dh, jnp.exp(-jax.nn.sigmoid(pre) * math.exp(-0.5)))
    loads[5].wait()
    spread(ah, jax.nn.sigmoid(rate_base[...] + dot(rate_low, rs[...])))
    loads[6].wait()
    rt[...] = turn(dot(normed, wr[...]).astype(BF).astype(F32))
    start_fetches(2)
    loads[7].start()

    block = math.gcd(count, 8)
    ones = jnp.ones((width, width), BF)
    lane = lax.broadcasted_iota(jnp.int32, (width, lanes), 1)

    def dot_split(values, right):
        flat = values.reshape(-1, values.shape[-1])
        high = flat.astype(BF)
        low = (flat - high.astype(F32)).astype(BF)
        return dot(high, right) + dot(low, right)

    def one_head(h, c):
        fetch(h).wait()
        k = kh[h]
        d = dh[h]
        unit = k * lax.rsqrt(jnp.sum(k * k, axis=-1, keepdims=True) + 1e-06)
        ua = unit * ah[h]
        rows = pl.ds(pl.multiple_of(h * width, width), width)
        v = vt[rows, :]
        r = rt[rows, :].astype(BF)
        tall = jnp.concatenate([k, jnp.zeros((lanes - count, width), F32)], axis=0).astype(BF)
        mixed = jnp.zeros((width, lanes), F32)
        for g in range(count // block):
            some = range(g * block, (g + 1) * block)

            def each(values):
                return jnp.stack([jnp.broadcast_to(values[b:b + 1], (width, width)) for b in some])

            s = st[h, g * block:(g + 1) * block]
            probe = dot_split(s * each(unit), ones).reshape(block, width, width)
            masked = jnp.concatenate([jnp.where(lane == b, v, 0.0) for b in some], axis=0)
            outer = dot(masked.astype(BF), tall).reshape(block, width, width)
            new = s * each(d) - probe * each(ua) + outer
            st[h, g * block:(g + 1) * block] = new
            got = dot_split(new, r).reshape(block, width, lanes)
            for i, b in enumerate(some):
                mixed = jnp.where(lane == b, got[i], mixed)
        put(h).start()
        centre = mixed - jnp.mean(mixed, axis=0, keepdims=True)
        var = jnp.mean(centre * centre, axis=0, keepdims=True)
        mt[rows, :] = centre * lax.rsqrt(var + 0.00064)
        return c

    lax.fori_loop(0, heads, one_head, 0)
    mixed = (mt[...].T[:count] * head_gain[...]).astype(BF)
    loads[7].wait()
    after = resid + dot(mixed, wo[...])
    after_ref[...] = after
    mean_sq = jnp.mean(after * after, axis=-1, keepdims=True)
    second = (after * lax.rsqrt(mean_sq + 1e-06) * second_gain[...]).astype(BF)
    part = second.shape[1] // (PARTS + 1)
    last = second[:, PARTS * part:]
    for j in range(PARTS):
        value = dot(table[PARTS], second[:, j * part:(j + 1) * part]) + dot(table[j], last)
        packed_ref[:, :, j * part:(j + 1) * part] = value.reshape(EXPERTS, ROWS, part).astype(BF)

    def end_put(h, c):
        put(h).wait()
        return c

    lax.fori_loop(0, heads, end_put, 0)


def mixer(args, order, share):
    (tokens, state, norm_gain, w_recept, w_keys, w_values, decay_base, d_first, d_second,
     rate_base, r_first, r_second, head_gain, w_output, second_gain) = args
    count, heads, width, _ = state.shape
    model = tokens.shape[1]
    part = model // (PARTS + 1)
    lanes = -(-count // 128) * 128
    vm = pl.BlockSpec(memory_space=pltpu.VMEM)
    hb = pl.BlockSpec(memory_space=pl.ANY)
    weights = [w_recept, w_keys, w_values, d_first, d_second, r_first, r_second, w_output]
    head_buf = pltpu.VMEM((heads, count, width), F32)
    return pl.pallas_call(
        mixer_kernel,
        out_shape=(
            jax.ShapeDtypeStruct(state.shape, F32),
            jax.ShapeDtypeStruct((count, model), F32),
            jax.ShapeDtypeStruct((EXPERTS, ROWS, PARTS * part), BF),
            jax.ShapeDtypeStruct((PARTS + 1, EXPERTS * ROWS, count), F32),
        ),
        in_specs=[vm] * 8 + [hb] * 9,
        out_specs=(hb, vm, vm, vm),
        scratch_shapes=[
            pltpu.VMEM((heads, count, width, width), F32),
            *[pltpu.VMEM(w.shape, w.dtype) for w in weights],
            head_buf, head_buf, head_buf,
            pltpu.VMEM((heads * width, lanes), F32),
            pltpu.VMEM((heads * width, lanes), F32),
            pltpu.VMEM((heads * width, lanes), F32),
            pltpu.SemaphoreType.DMA((8,)),
            pltpu.SemaphoreType.DMA((heads,)),
            pltpu.SemaphoreType.DMA((heads,)),
        ],
        compiler_params=pltpu.CompilerParams(vmem_limit_bytes=56 * 1024 * 1024),
        name="mixer",
    )(
        tokens, norm_gain[None], decay_base[None], rate_base[None], head_gain[None],
        second_gain[None], order, share, state, *weights,
    )


def expert_kernel(
    devices, packed, after, blend_w, unpack_m, pack_m, gate_h, up_h, down_h,
    out_ref,
    buf, rows_x, hidden, part_f, part_b, peer_b, zsend, ret, gate, up, down,
    w_sem, send1, recv1, fsend, frecv, ysend, yrecv, rsend, rrecv, own_sem,
):
    group = devices // EXPERTS
    me = lax.axis_index("ep")
    mine = me // group
    place = lax.rem(me, group)
    model = after.shape[1]
    part = model // (PARTS + 1)
    inner = gate.shape[1]
    step = math.gcd(inner, 256)

    loads = [
        pltpu.make_async_copy(src, dst, w_sem.at[i])
        for i, (src, dst) in enumerate([(gate_h, gate), (up_h, up), (down_h, down)])
    ]
    barrier = pltpu.get_barrier_semaphore()

    def other(i):
        return lax.rem(mine + i, EXPERTS)

    def peer(i):
        return lax.rem(place + i, group)

    def greet(i, c):
        pl.semaphore_signal(
            barrier, inc=1, device_id=(other(i) * group + place,), device_id_type=MESH
        )
        return c

    lax.fori_loop(1, EXPERTS, greet, 0)
    for i in range(1, group):
        pl.semaphore_signal(
            barrier, inc=1, device_id=(mine * group + peer(i),), device_id_type=MESH
        )
    for copy in loads:
        copy.start()
    pl.semaphore_wait(barrier, EXPERTS - 1 + group - 1)

    def dispatch(i):
        e = other(i)
        return pltpu.make_async_remote_copy(
            src_ref=packed.at[e], dst_ref=buf.at[place, mine],
            send_sem=send1.at[e], recv_sem=recv1.at[mine],
            device_id=(e * group + place,), device_id_type=MESH,
        )

    def arrive(s):
        return pltpu.make_async_remote_copy(
            src_ref=packed.at[s], dst_ref=buf.at[place, s],
            send_sem=send1.at[s], recv_sem=recv1.at[s],
            device_id=(s * group + place,), device_id_type=MESH,
        )

    def forward(s, i, src):
        q = peer(i)
        return pltpu.make_async_remote_copy(
            src_ref=src, dst_ref=buf.at[place, s],
            send_sem=fsend.at[i, s], recv_sem=frecv.at[place, s],
            device_id=(mine * group + q,), device_id_type=MESH,
        )

    def forwarded(s, i):
        q = peer(i)
        return pltpu.make_async_remote_copy(
            src_ref=buf.at[q, s], dst_ref=buf.at[q, s],
            send_sem=fsend.at[i, s], recv_sem=frecv.at[q, s],
            device_id=(mine * group + q,), device_id_type=MESH,
        )

    def start_dispatch(i, c):
        dispatch(i).start()
        return c

    lax.fori_loop(1, EXPERTS, start_dispatch, 0)
    own = pltpu.make_async_copy(packed.at[mine], buf.at[place, mine], own_sem.at[0])
    own.start()
    for i in range(1, group):
        forward(mine, i, packed.at[mine]).start()

    def relay(j, c):
        s = lax.rem(mine + EXPERTS - j, EXPERTS)
        arrive(s).wait_recv()
        for i in range(1, group):
            forward(s, i, buf.at[place, s]).start()
        return c

    lax.fori_loop(1, EXPERTS, relay, 0)
    own.wait()

    def end_relay(j, c):
        s = lax.rem(mine + EXPERTS - j, EXPERTS)
        for i in range(1, group):
            forwarded(s, i).wait_recv()
        return c

    lax.fori_loop(0, EXPERTS, end_relay, 0)

    packed_rows = EXPERTS * ROWS
    rows = EXPERTS * CAP_DEV
    for q in range(group):
        tail = jnp.zeros((rows, part), F32)
        for j in range(PARTS):
            cols = slice(j * part, (j + 1) * part)
            block = buf[q, :, :, cols].astype(F32).reshape(packed_rows, part).astype(BF)
            rows_x[q * rows:(q + 1) * rows, cols] = dot(unpack_m[PARTS], block).astype(BF)
            tail = tail + dot(unpack_m[j], block)
        rows_x[q * rows:(q + 1) * rows, PARTS * part:] = tail.astype(BF)

    loads[0].wait()
    loads[1].wait()

    def up_step(t, c):
        cols = pl.ds(pl.multiple_of(t * step, step), step)
        g = dot(rows_x[...], gate[:, cols])
        u = dot(rows_x[...], up[:, cols])
        hidden[:, cols] = (g * jax.nn.sigmoid(g) * u).astype(BF)
        return c

    lax.fori_loop(0, inner // step, up_step, 0)
    loads[2].wait()
    wide = math.gcd(model, 256)

    def down_step(t, c):
        cols = pl.ds(pl.multiple_of(t * wide, wide), wide)
        y = dot(hidden[...], down[:, cols])
        for q in range(group):
            mine_rows = y[q * rows:(q + 1) * rows]
            part_f[q, :, cols] = mine_rows
            part_b[q, :, cols] = mine_rows.astype(BF)
        return c

    lax.fori_loop(0, model // wide, down_step, 0)

    def swap(i):
        q = peer(i)
        return pltpu.make_async_remote_copy(
            src_ref=part_b.at[q], dst_ref=peer_b.at[place],
            send_sem=ysend.at[q], recv_sem=yrecv.at[place],
            device_id=(mine * group + q,), device_id_type=MESH,
        )

    def swapped(i):
        q = peer(i)
        return pltpu.make_async_remote_copy(
            src_ref=part_b.at[q], dst_ref=peer_b.at[q],
            send_sem=ysend.at[q], recv_sem=yrecv.at[q],
            device_id=(mine * group + q,), device_id_type=MESH,
        )

    for i in range(1, group):
        swap(i).start()
    for i in range(1, group):
        swapped(i).wait_recv()

    def summed(cols):
        total = part_f[place, :, cols]
        for i in range(1, group):
            total = total + peer_b[peer(i), :, cols].astype(F32)
        return total.astype(BF)

    last = summed(slice(PARTS * part, model))
    for j in range(PARTS):
        cols = slice(j * part, (j + 1) * part)
        value = dot(pack_m[PARTS], summed(cols)) + dot(pack_m[j], last)
        zsend[:, :, cols] = value.reshape(EXPERTS, ROWS, part).astype(BF)

    def give(i):
        e = other(i)
        return pltpu.make_async_remote_copy(
            src_ref=zsend.at[e], dst_ref=ret.at[mine],
            send_sem=rsend.at[e], recv_sem=rrecv.at[mine],
            device_id=(e * group + place,), device_id_type=MESH,
        )

    def take(s):
        return pltpu.make_async_remote_copy(
            src_ref=zsend.at[s], dst_ref=ret.at[s],
            send_sem=rsend.at[s], recv_sem=rrecv.at[s],
            device_id=(s * group + place,), device_id_type=MESH,
        )

    def start_give(i, c):
        give(i).start()
        return c

    lax.fori_loop(1, EXPERTS, start_give, 0)
    own_back = pltpu.make_async_copy(zsend.at[mine], ret.at[mine], own_sem.at[1])
    own_back.start()

    def drain(i, c):
        dispatch(i).wait_send()
        s = lax.rem(mine + EXPERTS - i, EXPERTS)
        for k in range(1, group):
            forwarded(s, k).wait_send()
        return c

    lax.fori_loop(1, EXPERTS, drain, 0)
    for i in range(1, group):
        forwarded(mine, i).wait_send()
        swap(i).wait_send()
    own_back.wait()

    def end_take(j, c):
        take(lax.rem(mine + EXPERTS - j, EXPERTS)).wait_recv()
        return c

    lax.fori_loop(1, EXPERTS, end_take, 0)

    def dot_turned(left, right):
        return lax.dot_general(left, right, (((0,), (0,)), ((), ())), preferred_element_type=F32)

    high = blend_w[...].astype(BF)
    low = (blend_w[...] - high.astype(F32)).astype(BF)
    tail = after[:, PARTS * part:]
    for j in range(PARTS):
        cols = slice(j * part, (j + 1) * part)
        block = ret[:, :, cols].astype(F32).reshape(packed_rows, part).astype(BF)
        value = after[:, cols] + dot_turned(high[PARTS], block) + dot_turned(low[PARTS], block)
        out_ref[:, cols] = value.astype(BF)
        tail = tail + dot_turned(high[j], block) + dot_turned(low[j], block)
    out_ref[:, PARTS * part:] = tail.astype(BF)

    def end_give(i, c):
        give(i).wait_send()
        return c

    lax.fori_loop(1, EXPERTS, end_give, 0)


def experts(packed, after, blend_w, gate, up, down, devices):
    group = devices // EXPERTS
    count, model = after.shape
    inner = gate.shape[1]
    rows = EXPERTS * CAP_DEV
    row = np.arange(rows)[:, None]
    place = np.arange(EXPERTS * ROWS)[None, :]
    same = row // CAP_DEV == place // ROWS
    slot, at = row % CAP_DEV, place % ROWS
    maps = [
        same & (at == CAP_DEV + slot // PARTS) & (slot % PARTS == j) for j in range(PARTS)
    ] + [same & (at == slot)]
    maps = np.stack(maps).astype(np.float32)
    unpack_m = jnp.asarray(maps, BF)
    pack_m = jnp.asarray(maps.transpose(0, 2, 1), BF)
    vm = pl.BlockSpec(memory_space=pltpu.VMEM)
    hb = pl.BlockSpec(memory_space=pl.ANY)
    wide = packed.shape[2]
    dma = pltpu.SemaphoreType.DMA
    return pl.pallas_call(
        functools.partial(expert_kernel, devices),
        out_shape=jax.ShapeDtypeStruct((count, model), BF),
        in_specs=[vm] * 5 + [hb] * 3,
        out_specs=vm,
        scratch_shapes=[
            pltpu.VMEM((group, EXPERTS, ROWS, wide), BF),
            pltpu.VMEM((group * rows, model), BF),
            pltpu.VMEM((group * rows, inner), BF),
            pltpu.VMEM((group, rows, model), F32),
            pltpu.VMEM((group, rows, model), BF),
            pltpu.VMEM((group, rows, model), BF),
            pltpu.VMEM((EXPERTS, ROWS, wide), BF),
            pltpu.VMEM((EXPERTS, ROWS, wide), BF),
            pltpu.VMEM(gate.shape, BF),
            pltpu.VMEM(up.shape, BF),
            pltpu.VMEM(down.shape, BF),
            dma((3,)),
            dma((EXPERTS,)),
            dma((EXPERTS,)),
            dma((group, EXPERTS)),
            dma((group, EXPERTS)),
            dma((group,)),
            dma((group,)),
            dma((EXPERTS,)),
            dma((EXPERTS,)),
            dma((2,)),
        ],
        compiler_params=pltpu.CompilerParams(
            collective_id=0, has_side_effects=True, vmem_limit_bytes=56 * 1024 * 1024
        ),
        name="experts",
    )(packed, after, blend_w, unpack_m, pack_m, gate, up, down)


def tables(route_ids, route_weights, rows_dev):
    start = lax.axis_index("ep") * rows_dev
    ids = lax.dynamic_slice_in_dim(route_ids, start, rows_dev, 0)
    weights = lax.dynamic_slice_in_dim(route_weights, start, rows_dev, 0)
    hit = ids[None, :, :] == jnp.arange(EXPERTS, dtype=jnp.int32)[:, None, None]
    member = jnp.any(hit, axis=2)
    share = jnp.sum(jnp.where(hit, weights[None, :, :], 0.0), axis=2)
    order = jnp.cumsum(member.astype(jnp.int32), axis=1) - 1
    return jnp.where(member, order, -1), share


def on_device(
    tokens, state, norm_gain, w_recept, w_keys, w_values, decay_base, decay_first_matrix,
    decay_second_matrix, rate_base, rate_first_matrix, rate_second_matrix, head_gain, w_output,
    second_gain, route_ids, route_weights, expert_gate, expert_up, expert_down,
):
    devices = lax.axis_size("ep")
    order, share = tables(route_ids, route_weights, tokens.shape[0])
    new_state, after, packed, blend_w = mixer(
        (tokens, state, norm_gain, w_recept, w_keys, w_values, decay_base, decay_first_matrix,
         decay_second_matrix, rate_base, rate_first_matrix, rate_second_matrix, head_gain,
         w_output, second_gain),
        order,
        share,
    )
    layer_out = experts(packed, after, blend_w, expert_gate, expert_up, expert_down, devices)
    return (layer_out, new_state)


def solution(mesh):
    rep = P()
    in_specs = (
        P("ep", None), P("ep", None, None, None), *[rep] * 15,
        P(None, "ep"), P(None, "ep"), P("ep", None),
    )
    out_specs = (P("ep", None), P("ep", None, None, None))
    return jax.shard_map(
        on_device, mesh=mesh, in_specs=in_specs, out_specs=out_specs, check_vma=False
    )
```

profile of v0, /device:TPU:0, one launch (start us, length us, event | category | flops | bytes accessed | tf_op | source)
XLA Modules:
  0.0 69.5 jit_solution(17296721655529367562)
XLA Ops:
  0.6 0.0 copy-start
  0.6 0.7 copy-done
  1.3 0.1 constant_dynamic-slice_fusion.1
  1.4 0.8 %constant_dynamic-slice_fusion = f32[24,2]{0,1:T(2,128)S(1)} fusion(f32[768,2]{0,1:T(2,128)} %param.38, s32[]{:T(128)S(6)} %select_n.12), kind=kLoop, calls=%fused_computation.4 | loop fusion | bytes 388 | tf_op jit(solution)/shard_map/dynamic_slice | solution.py:500
  2.2 0.6 select_reduce_fusion.share
  2.8 0.2 reduce_window_sum.11
  2.9 0.6 add_select_fusion.order
  3.6 27.4 %mixer.1 = (f32[24,16,64,64]{3,2,1,0:T(8,128)}, f32[24,2048]{1,0:T(8,128)}, bf16[16,8,1536]{2,1,0:T(8,128)(2,1)}, f32[4,128,24]{2,1,0:T(8,128)}) custom-call(bf16[24,2048]{1,0:T(8,128)(2,1)} %tokens.1, f32[1,2048]{1,0:T(1,128)} %bitcast.5, f32[1,1024]{1,0:T(1,128)} %bitcast.7, f32[1,1024]{1,0:T(1,128)} %bitcast.8, f32[1,1024]{1,0:T(1,128)} %bitcast.9, ...), custom_call_target="tpu_custom_call" | custom-call | tf_op jit(solution)/shard_map/mixer/pallas_call | solution.py:181
  30.9 37.0 %experts.1 = bf16[24,2048]{1,0:T(8,128)(2,1)} custom-call(bf16[16,8,1536]{2,1,0:T(8,128)(2,1)} %get-tuple-element.6.packed, f32[24,2048]{1,0:T(8,128)} %get-tuple-element.7.after, f32[4,128,24]{2,1,0:T(8,128)} %get-tuple-element.8.blend_w, bf16[4,96,128]{2,1,0:T(8,128)(2,1)} %constant.25.clone.unpack_m, bf16[4,128,96]{2,1,0:T(8,128)(2,1)} %constant.26.clone.pack_m, ...), custom_call_target="tpu_custom_call" | custom-call | tf_op jit(solution)/shard_map/experts/pallas_call | solution.py:462
  68.0 1.5 %copy.27 = bf16[24,2048]{1,0:T(8,128)(2,1)} copy(bf16[24,2048]{1,0:T(8,128)(2,1)} %experts.1) | data formatting | bytes 196608
  (2 shorter events, 0.0 us)
Async XLA Ops:
  0.6 0.7 %copy-start = (s32[768,2]{0,1:T(2,128)S(1)}, s32[768,2]{0,1:T(2,128)}, u32[]{:S(2)}) copy-start(s32[768,2]{0,1:T(2,128)} %param.37) | copy-start | bytes 18436
where the time goes:
time: 70.1 us; the launch traced here: 69.5 us
  Pallas kernels  64.4 us (92%)
  local copies, waits for them, and re-layouts  3.05 us (4%)
  other arithmetic  1.39 us (2%)
    pallas_call x1, Pallas kernels, experts(): pl.pallas_call(functools.partial(expert_kernel, devices), out_shape=jax.S...  37 us
    pallas_call x1, Pallas kernels, mixer(): pl.pallas_call(mixer_kernel, out_shape=(jax.ShapeDtypeStruct(state.shape,...  27.4 us
    unnamed x3, local copies, waits for them, and re-layouts  2.23 us

commit v1 on v0

v1 whole, which is shorter than its diff:
```python
import functools
import math

import jax
import jax.numpy as jnp
import numpy as np
from jax import lax
from jax.experimental import pallas as pl
from jax.experimental.pallas import tpu as pltpu
from jax.sharding import PartitionSpec as P

EXPERTS = 16
CAP_DEV = 6
ROWS = 8
PARTS = 3
LANES = 128
STRIDE = 32
MIX_CHUNKS = 2
OUT_CHUNKS = 4
MESH = pl.DeviceIdType.MESH
BF = jnp.bfloat16
F32 = jnp.float32


def dot(a, b):
    return jnp.dot(a, b, preferred_element_type=F32)


def split(values):
    high = values.astype(BF)
    return high, (values - high.astype(F32)).astype(BF)


def layer_kernel(
    devices,
    tokens, norm_gain, decay_base, rate_base, head_gain, second_gain, ids, shares, unpack_m, pack_m,
    state, w_recept, w_keys, w_values, d_first, d_second, r_first, r_second, w_output,
    gate_h, up_h, down_h,
    st, ret_out, after_ref, blend_ref,
    wr, wk, wv, df, ds, rf, rs, wo, gate, up, down,
    table, rowbuf, dh, w2, turned, pq, pv, mixed_ref,
    tok_send, tok_buf, mix_send, mix_buf, own_rows, rows_x, hidden,
    part_f, part_b, peer_b, zsend, ret,
    w_sem, in_sem, tsend, trecv, msend, mrecv, xsend, xrecv, ysend, yrecv, rsend, rrecv,
):
    heads, count, width, _ = st.shape
    model = tokens.shape[1]
    inner_mix = heads * width
    group = devices // EXPERTS
    me = lax.axis_index("ep")
    mine = lax.div(me, group)
    place = lax.rem(me, group)
    packed_rows = EXPERTS * ROWS
    rows = EXPERTS * CAP_DEV

    order_of = [
        (d_first, df), (r_first, rf), (w_keys, wk), (w_values, wv), (d_second, ds),
        (r_second, rs), (w_recept, wr), (w_output, wo), (gate_h, gate), (up_h, up), (down_h, down),
    ]
    loads = [
        pltpu.make_async_copy(src, dst, w_sem.at[i]) for i, (src, dst) in enumerate(order_of)
    ]
    for i in (0, 1, 2, 3):
        loads[i].start()

    def other(i):
        total = 0
        for k in range(EXPERTS.bit_length() - 1):
            a = lax.rem(lax.div(mine, 1 << k), 2)
            b = lax.rem(lax.div(i, 1 << k), 2)
            total = total + (a + b - 2 * a * b) * (1 << k)
        return total

    def each_other(body):
        def step(j, c):
            body(other(EXPERTS - j))
            return c

        lax.fori_loop(1, EXPERTS, step, 0)

    def peer(i):
        return lax.rem(place + i, group)

    barrier = pltpu.get_barrier_semaphore()

    def greet(e):
        pl.semaphore_signal(barrier, inc=1, device_id=(e * group + place,), device_id_type=MESH)

    each_other(greet)
    for i in range(1, group):
        pl.semaphore_signal(
            barrier, inc=1, device_id=(mine * group + peer(i),), device_id_type=MESH
        )

    def fetch(h):
        return pltpu.make_async_copy(state.at[:, h], st.at[h], in_sem.at[h])

    def start_fetches(low, high):
        def step(h, c):
            fetch(h).start()
            return c

        lax.fori_loop(low, high, step, 0)

    total_rows = ids.shape[1]
    spot = lax.broadcasted_iota(jnp.int32, (total_rows, count), 0)
    column = lax.broadcasted_iota(jnp.int32, (total_rows, count), 1)
    choose = jnp.where(spot == column + me * count, 1.0, 0.0).astype(BF)
    my_ids = dot(ids[...].astype(F32).astype(BF), choose)
    share_high, share_low = split(shares[...])
    my_shares = dot(share_high, choose) + dot(share_low, choose)
    expert_at = lax.broadcasted_iota(jnp.int32, (EXPERTS, count), 0).astype(F32)
    member = jnp.zeros((EXPERTS, count), F32)
    share = jnp.zeros((EXPERTS, count), F32)
    for k in range(ids.shape[0]):
        hit = jnp.where(expert_at == my_ids[k:k + 1], 1.0, 0.0)
        member = member + hit
        share = share + hit * my_shares[k:k + 1]
    earlier = jnp.where(
        lax.broadcasted_iota(jnp.int32, (count, count), 0)
        < lax.broadcasted_iota(jnp.int32, (count, count), 1),
        1.0, 0.0,
    ).astype(BF)
    order = jnp.where(member > 0.5, dot(member.astype(BF), earlier), -1.0)
    shape = (EXPERTS, ROWS, count)
    slot = jnp.broadcast_to(order[:, None, :], shape)
    weight = jnp.broadcast_to(share[:, None, :], shape)
    at = lax.broadcasted_iota(jnp.int32, shape, 1).astype(F32)
    for j in range(PARTS + 1):
        if j == PARTS:
            hits = (slot == at) & (at < CAP_DEV)
        else:
            hits = (slot == (at - CAP_DEV) * PARTS + j) & (at >= CAP_DEV)
        hits = jnp.where(hits, 1.0, 0.0)
        blend_ref[j] = (hits * weight).reshape(packed_rows, count)
        table[j] = hits.reshape(packed_rows, count).astype(BF)

    def pack(values, put):
        part = values.shape[1] // (PARTS + 1)
        last = values[:, PARTS * part:]
        for j in range(PARTS):
            value = dot(table[PARTS], values[:, j * part:(j + 1) * part]) + dot(table[j], last)
            put(slice(j * part, (j + 1) * part), value.reshape(EXPERTS, ROWS, part).astype(BF))

    def put_tokens(cols, value):
        tok_send[:, :, cols] = value

    pack(tokens[...], put_tokens)
    tok_buf[mine] = tok_send[mine]

    def give_tokens(e):
        return pltpu.make_async_remote_copy(
            src_ref=tok_send.at[e], dst_ref=tok_buf.at[mine],
            send_sem=tsend.at[e], recv_sem=trecv.at[mine],
            device_id=(e * group + place,), device_id_type=MESH,
        )

    def take_tokens(s):
        return pltpu.make_async_remote_copy(
            src_ref=tok_send.at[s], dst_ref=tok_buf.at[s],
            send_sem=tsend.at[s], recv_sem=trecv.at[s],
            device_id=(s * group + place,), device_id_type=MESH,
        )

    pl.semaphore_wait(barrier, EXPERTS - 1 + group - 1)
    each_other(lambda e: give_tokens(e).start())

    resid = tokens[...].astype(F32)
    mean_sq = jnp.mean(resid * resid, axis=-1, keepdims=True)
    normed = (resid * lax.rsqrt(mean_sq + 1e-06) * norm_gain[...]).astype(BF)
    loads[0].wait()
    decay_low = jnp.tanh(dot(normed, df[...])).astype(BF)
    loads[1].wait()
    rate_low = dot(normed, rf[...]).astype(BF)
    loads[2].wait()
    k = dot(normed, wk[...]).astype(BF).astype(F32)
    for i in (4, 5, 6):
        loads[i].start()
    loads[3].wait()
    v = dot(normed, wv[...]).astype(BF).astype(F32)
    start_fetches(0, heads // 2)
    loads[4].wait()
    pre = decay_base[...] + dot(decay_low, ds[...])
    d = jnp.exp(-jax.nn.sigmoid(pre) * math.exp(-0.5))
    loads[5].wait()
    a = jax.nn.sigmoid(rate_base[...] + dot(rate_low, rs[...]))
    loads[6].wait()
    start_fetches(heads // 2, heads)
    r = dot(normed, wr[...]).astype(BF).astype(F32)

    same_head = (
        lax.broadcasted_iota(jnp.int32, (LANES, LANES), 0) // width
        == lax.broadcasted_iota(jnp.int32, (LANES, LANES), 1) // width
    )

    def head_sums(values, scale):
        ones = jnp.where(same_head, scale, 0.0).astype(BF)
        high, low = split(values)
        tiles = [slice(t, t + LANES) for t in range(0, values.shape[1], LANES)]
        return jnp.concatenate([dot(high[:, t], ones) + dot(low[:, t], ones) for t in tiles], axis=1)

    sums = head_sums(jnp.concatenate([k * k, k * a * r, k * r], axis=0), 1.0)
    scale = lax.rsqrt(sums[:count] + 1e-06)
    unit = k * scale
    toward = d * r - unit * (sums[count:2 * count] * scale)
    rowbuf[0] = d
    rowbuf[1] = -unit * a
    rowbuf[2] = k
    rowbuf[3] = v * sums[2 * count:]
    gap = jnp.zeros((STRIDE - count, inner_mix), F32)
    tall = jnp.concatenate(
        [unit, gap, toward, gap, jnp.zeros((STRIDE, inner_mix), F32), v, gap], axis=0
    )
    turned[...] = tall.T.astype(BF)

    block = math.gcd(count, 8)
    lane = lax.broadcasted_iota(jnp.int32, (width, LANES), 1)
    lane_of = lax.rem(lane, STRIDE)

    def first_pass(h, c):
        fetch(h).wait()
        span = pl.ds(pl.multiple_of(h * width, width), width)
        right = turned[span, :]
        acc = jnp.zeros((width, LANES), F32)
        for g in range(count // block):
            s = st[h, g * block:(g + 1) * block]
            got = dot(s.reshape(block * width, width).astype(BF), right)
            got = got.reshape(block, width, LANES)
            for i in range(block):
                acc = jnp.where(lane_of == g * block + i, got[i], acc)
        pq[span, :] = acc
        pv[span, :] = jnp.where(lane < STRIDE, acc, right.astype(F32))
        return c

    wide = inner_mix // MIX_CHUNKS
    half = heads // MIX_CHUNKS

    def give_mixed(n, e):
        return pltpu.make_async_remote_copy(
            src_ref=mix_send.at[n, e], dst_ref=mix_buf.at[n, mine],
            send_sem=msend.at[n, e], recv_sem=mrecv.at[n, mine],
            device_id=(e * group + place,), device_id_type=MESH,
        )

    def take_mixed(n, s):
        return pltpu.make_async_remote_copy(
            src_ref=mix_send.at[n, s], dst_ref=mix_buf.at[n, s],
            send_sem=msend.at[n, s], recv_sem=mrecv.at[n, s],
            device_id=(s * group + place,), device_id_type=MESH,
        )

    def mix_chunk(n):
        lax.fori_loop(n * half, (n + 1) * half, first_pass, 0)
        cols = slice(n * wide, (n + 1) * wide)
        mixed = pq[cols, :].T[STRIDE:STRIDE + count] + rowbuf[3, :, cols]
        centre = mixed - head_sums(mixed, 1.0 / width)
        var = head_sums(centre * centre, 1.0 / width)
        out = (centre * lax.rsqrt(var + 0.00064) * head_gain[:, cols]).astype(BF)
        mixed_ref[:, cols] = out

        def put(at_cols, value):
            mix_send[n, :, :, at_cols] = value

        pack(out, put)
        mix_buf[n, mine] = mix_send[n, mine]
        each_other(lambda e: give_mixed(n, e).start())

    def unpack(source, m, width_of):
        part = width_of // (PARTS + 1)
        pieces, tail = [], jnp.zeros((rows, part), F32)
        for j in range(PARTS):
            value = source(slice(j * part, (j + 1) * part))
            value = value.astype(F32).reshape(packed_rows, part).astype(BF)
            pieces.append(dot(m[PARTS], value))
            tail = tail + dot(m[j], value)
        return pieces + [tail]

    mix_chunk(0)
    loads[7].start()
    loads[8].start()
    mix_chunk(1)
    loads[9].start()
    loads[10].start()

    each_other(lambda s: take_tokens(s).wait_recv())
    for j, piece in enumerate(unpack(lambda cols: tok_buf[:, :, cols], unpack_m, model)):
        part = model // (PARTS + 1)
        own_rows[:, j * part:(j + 1) * part] = piece

    for h in range(heads):
        cols = slice(h * width, (h + 1) * width)
        dh[h] = rowbuf[0, :, cols]
        w2[h] = jnp.concatenate(
            [
                rowbuf[1, :, cols], jnp.zeros((3 * STRIDE - count, width), F32),
                rowbuf[2, :, cols], jnp.zeros((STRIDE - count, width), F32),
            ],
            axis=0,
        ).astype(BF)

    def second_pass(h, c):
        span = pl.ds(pl.multiple_of(h * width, width), width)
        left = pv[span, :]
        right = w2[h]
        decay = dh[h]
        for g in range(count // block):
            some = range(g * block, (g + 1) * block)
            masked = jnp.concatenate([jnp.where(lane_of == b, left, 0.0) for b in some], axis=0)
            change = dot(masked.astype(BF), right).reshape(block, width, width)
            by = jnp.stack([jnp.broadcast_to(decay[b:b + 1], (width, width)) for b in some])
            st[h, g * block:(g + 1) * block] = st[h, g * block:(g + 1) * block] * by + change
        return c

    lax.fori_loop(0, heads, second_pass, 0)

    loads[7].wait()
    step_out = math.gcd(model, 256)

    def add_mixed(n):
        each_other(lambda s: take_mixed(n, s).wait_recv())
        pieces = unpack(lambda cols: mix_buf[n, :, :, cols], unpack_m, wide)
        got = jnp.concatenate(pieces, axis=1).astype(BF)

        def step(t, c):
            cols = pl.ds(pl.multiple_of(t * step_out, step_out), step_out)
            own_rows[:, cols] = own_rows[:, cols] + dot(got, wo[n * wide:(n + 1) * wide, cols])
            return c

        lax.fori_loop(0, model // step_out, step, 0)

    for n in range(MIX_CHUNKS):
        add_mixed(n)

    def second_norm(values):
        mean_of = jnp.mean(values * values, axis=-1, keepdims=True)
        return (values * lax.rsqrt(mean_of + 1e-06) * second_gain[...]).astype(BF)

    rows_x[place] = second_norm(own_rows[...])

    def share_rows(i):
        return pltpu.make_async_remote_copy(
            src_ref=rows_x.at[place], dst_ref=rows_x.at[place],
            send_sem=xsend.at[peer(i)], recv_sem=xrecv.at[place],
            device_id=(mine * group + peer(i),), device_id_type=MESH,
        )

    def shared_rows(i):
        return pltpu.make_async_remote_copy(
            src_ref=rows_x.at[peer(i)], dst_ref=rows_x.at[peer(i)],
            send_sem=xsend.at[peer(i)], recv_sem=xrecv.at[peer(i)],
            device_id=(mine * group + peer(i),), device_id_type=MESH,
        )

    for i in range(1, group):
        share_rows(i).start()

    def after_step(t, c):
        cols = pl.ds(pl.multiple_of(t * step_out, step_out), step_out)
        after_ref[:, cols] = tokens[:, cols].astype(F32) + dot(mixed_ref[...], wo[:, cols])
        return c

    lax.fori_loop(0, model // step_out, after_step, 0)
    loads[8].wait()
    loads[9].wait()
    for i in range(1, group):
        shared_rows(i).wait_recv()

    inner = gate.shape[1]
    step_in = math.gcd(inner, 256)

    def up_step(t, c):
        cols = pl.ds(pl.multiple_of(t * step_in, step_in), step_in)
        left = rows_x[...].reshape(group * rows, model)
        g = dot(left, gate[:, cols])
        u = dot(left, up[:, cols])
        hidden[:, cols] = (g * jax.nn.sigmoid(g) * u).astype(BF)
        return c

    lax.fori_loop(0, inner // step_in, up_step, 0)
    loads[10].wait()
    chunk = model // OUT_CHUNKS
    small = math.gcd(chunk, 256)

    def swap(n, i):
        q = peer(i)
        return pltpu.make_async_remote_copy(
            src_ref=part_b.at[n, q], dst_ref=peer_b.at[n, place],
            send_sem=ysend.at[n, q], recv_sem=yrecv.at[n, place],
            device_id=(mine * group + q,), device_id_type=MESH,
        )

    def swapped(n, i):
        q = peer(i)
        return pltpu.make_async_remote_copy(
            src_ref=part_b.at[n, q], dst_ref=peer_b.at[n, q],
            send_sem=ysend.at[n, q], recv_sem=yrecv.at[n, q],
            device_id=(mine * group + q,), device_id_type=MESH,
        )

    def down_chunk(n, c):
        for t in range(chunk // small):
            cols = pl.ds(pl.multiple_of(n * chunk + t * small, small), small)
            y = dot(hidden[...], down[:, cols])
            for q in range(group):
                piece = y[q * rows:(q + 1) * rows]
                part_f[n, q, :, t * small:(t + 1) * small] = piece
                part_b[n, q, :, t * small:(t + 1) * small] = piece.astype(BF)
        for i in range(1, group):
            swap(n, i).start()
        return c

    lax.fori_loop(0, OUT_CHUNKS, down_chunk, 0)

    def give(n, e):
        return pltpu.make_async_remote_copy(
            src_ref=zsend.at[n, e], dst_ref=ret.at[n, mine],
            send_sem=rsend.at[n, e], recv_sem=rrecv.at[n, mine],
            device_id=(e * group + place,), device_id_type=MESH,
        )

    def take(n, s):
        return pltpu.make_async_remote_copy(
            src_ref=zsend.at[n, s], dst_ref=ret.at[n, s],
            send_sem=rsend.at[n, s], recv_sem=rrecv.at[n, s],
            device_id=(s * group + place,), device_id_type=MESH,
        )

    part = chunk // (PARTS + 1)

    def return_chunk(n, c):
        for i in range(1, group):
            swapped(n, i).wait_recv()

        def summed(cols):
            total = part_f[n, place, :, cols]
            for i in range(1, group):
                total = total + peer_b[n, peer(i), :, cols].astype(F32)
            return total.astype(BF)

        last = summed(slice(PARTS * part, chunk))
        for j in range(PARTS):
            cols = slice(j * part, (j + 1) * part)
            value = dot(pack_m[PARTS], summed(cols)) + dot(pack_m[j], last)
            zsend[n, :, :, cols] = value.reshape(EXPERTS, ROWS, part).astype(BF)
        ret[n, mine] = zsend[n, mine]
        each_other(lambda e: give(n, e).start())
        return c

    lax.fori_loop(0, OUT_CHUNKS, return_chunk, 0)

    def end_sends(e):
        give_tokens(e).wait_send()
        for n in range(MIX_CHUNKS):
            give_mixed(n, e).wait_send()

    each_other(end_sends)
    for i in range(1, group):
        share_rows(i).wait_send()

    def end_chunk(n, c):
        for i in range(1, group):
            swap(n, i).wait_send()
        each_other(lambda s: take(n, s).wait_recv())
        ret_out[n] = ret[n]
        return c

    lax.fori_loop(0, OUT_CHUNKS, end_chunk, 0)

    def end_give(n, c):
        each_other(lambda e: give(n, e).wait_send())
        return c

    lax.fori_loop(0, OUT_CHUNKS, end_give, 0)


def finish_kernel(st, ret, after, blend_w, new_state, layer_out, out, sem, out_sem):
    heads = st.shape[0]

    def put(h):
        return pltpu.make_async_copy(st.at[h], new_state.at[:, h], sem.at[h])

    def start(h, c):
        put(h).start()
        return c

    lax.fori_loop(0, heads, start, 0)

    def dot_turned(left, right):
        return lax.dot_general(left, right, (((0,), (0,)), ((), ())), preferred_element_type=F32)

    high, low = split(blend_w[...])
    chunk = after.shape[1] // OUT_CHUNKS
    part = chunk // (PARTS + 1)
    packed_rows = EXPERTS * ROWS
    for n in range(OUT_CHUNKS):
        tail_at = slice(n * chunk + PARTS * part, (n + 1) * chunk)
        tail = after[:, tail_at]
        for j in range(PARTS):
            cols = slice(n * chunk + j * part, n * chunk + (j + 1) * part)
            block = ret[n, :, :, j * part:(j + 1) * part]
            block = block.astype(F32).reshape(packed_rows, part).astype(BF)
            value = after[:, cols] + dot_turned(high[PARTS], block) + dot_turned(low[PARTS], block)
            out[:, cols] = value.astype(BF)
            tail = tail + dot_turned(high[j], block) + dot_turned(low[j], block)
        out[:, tail_at] = tail.astype(BF)
    last = pltpu.make_async_copy(out, layer_out, out_sem.at[0])
    last.start()

    def end(h, c):
        put(h).wait()
        return c

    lax.fori_loop(0, heads, end, 0)
    last.wait()


def maps():
    rows = EXPERTS * CAP_DEV
    row = np.arange(rows)[:, None]
    place = np.arange(EXPERTS * ROWS)[None, :]
    same = row // CAP_DEV == place // ROWS
    slot, at = row % CAP_DEV, place % ROWS
    found = [
        same & (at == CAP_DEV + slot // PARTS) & (slot % PARTS == j) for j in range(PARTS)
    ] + [same & (at == slot)]
    found = np.stack(found).astype(np.float32)
    return jnp.asarray(found, BF), jnp.asarray(found.transpose(0, 2, 1), BF)


def on_device(
    tokens, state, norm_gain, w_recept, w_keys, w_values, decay_base, decay_first_matrix,
    decay_second_matrix, rate_base, rate_first_matrix, rate_second_matrix, head_gain, w_output,
    second_gain, route_ids, route_weights, expert_gate, expert_up, expert_down,
):
    devices = lax.axis_size("ep")
    group = devices // EXPERTS
    count, heads, width, _ = state.shape
    model = tokens.shape[1]
    inner = expert_gate.shape[1]
    mix = heads * width
    rows = EXPERTS * CAP_DEV
    packed_rows = EXPERTS * ROWS
    folded = PARTS * model // (PARTS + 1)
    mix_fold = PARTS * (mix // MIX_CHUNKS) // (PARTS + 1)
    out_fold = PARTS * (model // OUT_CHUNKS) // (PARTS + 1)
    unpack_m, pack_m = maps()
    vm = pl.BlockSpec(memory_space=pltpu.VMEM)
    hb = pl.BlockSpec(memory_space=pl.ANY)
    dma = pltpu.SemaphoreType.DMA
    weights = [
        w_recept, w_keys, w_values, decay_first_matrix, decay_second_matrix, rate_first_matrix,
        rate_second_matrix, w_output, expert_gate, expert_up, expert_down,
    ]
    st, ret, after, blend_w = pl.pallas_call(
        functools.partial(layer_kernel, devices),
        out_shape=(
            pltpu.VMEM((heads, count, width, width), F32),
            pltpu.VMEM((OUT_CHUNKS, EXPERTS, ROWS, out_fold), BF),
            pltpu.VMEM((count, model), F32),
            pltpu.VMEM((PARTS + 1, packed_rows, count), F32),
        ),
        in_specs=[vm] * 10 + [hb] * 12,
        out_specs=(vm, vm, vm, vm),
        scratch_shapes=[
            *[pltpu.VMEM(w.shape, BF) for w in weights],
            pltpu.VMEM((PARTS + 1, packed_rows, count), BF),
            pltpu.VMEM((4, count, mix), F32),
            pltpu.VMEM((heads, count, width), F32),
            pltpu.VMEM((heads, LANES, width), BF),
            pltpu.VMEM((mix, LANES), BF),
            pltpu.VMEM((mix, LANES), F32),
            pltpu.VMEM((mix, LANES), F32),
            pltpu.VMEM((count, mix), BF),
            pltpu.VMEM((EXPERTS, ROWS, folded), BF),
            pltpu.VMEM((EXPERTS, ROWS, folded), BF),
            pltpu.VMEM((MIX_CHUNKS, EXPERTS, ROWS, mix_fold), BF),
            pltpu.VMEM((MIX_CHUNKS, EXPERTS, ROWS, mix_fold), BF),
            pltpu.VMEM((rows, model), F32),
            pltpu.VMEM((group, rows, model), BF),
            pltpu.VMEM((group * rows, inner), BF),
            pltpu.VMEM((OUT_CHUNKS, group, rows, model // OUT_CHUNKS), F32),
            pltpu.VMEM((OUT_CHUNKS, group, rows, model // OUT_CHUNKS), BF),
            pltpu.VMEM((OUT_CHUNKS, group, rows, model // OUT_CHUNKS), BF),
            pltpu.VMEM((OUT_CHUNKS, EXPERTS, ROWS, out_fold), BF),
            pltpu.VMEM((OUT_CHUNKS, EXPERTS, ROWS, out_fold), BF),
            dma((len(weights),)),
            dma((heads,)),
            dma((EXPERTS,)),
            dma((EXPERTS,)),
            dma((MIX_CHUNKS, EXPERTS)),
            dma((MIX_CHUNKS, EXPERTS)),
            dma((group,)),
            dma((group,)),
            dma((OUT_CHUNKS, group)),
            dma((OUT_CHUNKS, group)),
            dma((OUT_CHUNKS, EXPERTS)),
            dma((OUT_CHUNKS, EXPERTS)),
        ],
        compiler_params=pltpu.CompilerParams(
            collective_id=0, has_side_effects=True, vmem_limit_bytes=49 * 1024 * 1024
        ),
        name="layer",
    )(
        tokens, norm_gain[None], decay_base[None], rate_base[None], head_gain[None],
        second_gain[None], route_ids.T, route_weights.T, unpack_m, pack_m, state, w_recept, w_keys,
        w_values, decay_first_matrix, decay_second_matrix, rate_first_matrix, rate_second_matrix,
        w_output, expert_gate, expert_up, expert_down,
    )
    new_state, layer_out = pl.pallas_call(
        finish_kernel,
        out_shape=(
            jax.ShapeDtypeStruct(state.shape, F32),
            jax.ShapeDtypeStruct((count, model), BF),
        ),
        in_specs=[vm] * 4,
        out_specs=(hb, hb),
        scratch_shapes=[pltpu.VMEM((count, model), BF), dma((heads,)), dma((1,))],
        compiler_params=pltpu.CompilerParams(vmem_limit_bytes=4 * 1024 * 1024),
        name="finish",
    )(st, ret, after, blend_w)
    return (layer_out, new_state)


def solution(mesh):
    rep = P()
    in_specs = (
        P("ep", None), P("ep", None, None, None), *[rep] * 15,
        P(None, "ep"), P(None, "ep"), P("ep", None),
    )
    out_specs = (P("ep", None), P("ep", None, None, None))
    return jax.shard_map(
        on_device, mesh=mesh, in_specs=in_specs, out_specs=out_specs, check_vma=False
    )
```

time: 70.1 us -> 54.7 us (0.78)
  Pallas kernels: 64.4 us -> 53.9 us
  local copies, waits for them, and re-layouts: 3.05 us -> 0 us
  other arithmetic: 1.39 us -> 0 us
    pallas_call x2, Pallas kernels: 64.4 us -> 53.9 us  [the longest x1 49.2 us: on_device(): pl.pallas_call(functools.partial(layer_kernel, devices), out_shape=(pltpu...]
    unnamed x3 -> x0, local copies, waits for them, and re-layouts: 2.23 us -> none
    dynamic_slice x2 -> x0, local copies, waits for them, and re-layouts: 0.83 us -> none  [the longest x1 0.75 us: tables(): weights = lax.dynamic_slice_in_dim(route_weights, start, rows_dev, 0)]
where the time goes in v1:
time: 54.7 us; the launch traced here: 54.6 us
  Pallas kernels  53.9 us (99%)
  between operations  0.65 us (1%)
    pallas_call x1, Pallas kernels, on_device(): pl.pallas_call(functools.partial(layer_kernel, devices), out_shape=(pltpu...  49.2 us
    pallas_call x1, Pallas kernels, on_device(): pl.pallas_call(finish_kernel, out_shape=(jax.ShapeDtypeStruct(state.shape...  4.72 us

profile of v1, /device:TPU:0, one launch (start us, length us, event | category | flops | bytes accessed | tf_op | source)
XLA Modules:
  0.0 54.6 jit_solution(17461988516312076730)
XLA Ops:
  0.6 49.2 %layer.1 = (f32[16,24,64,64]{3,2,1,0:T(8,128)S(1)}, bf16[4,16,8,384]{3,2,1,0:T(8,128)(2,1)S(1)}, f32[24,2048]{1,0:T(8,128)S(1)}, f32[4,128,24]{2,1,0:T(8,128)S(1)}) custom-call(bf16[24,2048]{1,0:T(8,128)(2,1)} %tokens.1, f32[1,2048]{1,0:T(1,128)} %bitcast.7, f32[1,1024]{1,0:T(1,128)} %bitcast.11, f32[1,1024]{1,0:T(1,128)} %bitcast.12, f32[1,1024]{1,0:T(1,128)} %bitcast.13, ...), custom_call_target="tpu_custom_call" | custom-call | tf_op jit(solution)/shard_map/layer/pallas_call | solution.py:554
  49.9 4.7 %finish.1 = (f32[24,16,64,64]{3,2,1,0:T(8,128)}, bf16[24,2048]{1,0:T(8,128)(2,1)}) custom-call(f32[16,24,64,64]{3,2,1,0:T(8,128)S(1)} %get-tuple-element.8.st, bf16[4,16,8,384]{3,2,1,0:T(8,128)(2,1)S(1)} %get-tuple-element.9.ret, f32[24,2048]{1,0:T(8,128)S(1)} %get-tuple-element.10.after, f32[4,128,24]{2,1,0:T(8,128)S(1)} %get-tuple-element.11.blend_w), custom_call_target="tpu_custom_call" | custom-call | tf_op jit(solution)/shard_map/finish/pallas_call | solution.py:609

commit v2 on v1

v2 whole, which is shorter than its diff:
```python
import functools
import math

import jax
import jax.numpy as jnp
import numpy as np
from jax import lax
from jax.experimental import pallas as pl
from jax.experimental.pallas import tpu as pltpu
from jax.sharding import PartitionSpec as P

EXPERTS = 16
CAP_DEV = 6
ROWS = 8
PARTS = 3
LANES = 128
STRIDE = 32
MIX_CHUNKS = 2
OUT_CHUNKS = 4
PAIRS_AT_ONCE = 2
LAG = 3
BESIDE = (8, 4)
MESH = pl.DeviceIdType.MESH
BF = jnp.bfloat16
F32 = jnp.float32


def dot(a, b):
    return jnp.dot(a, b, preferred_element_type=F32)


def split(values):
    high = values.astype(BF)
    return high, (values - high.astype(F32)).astype(BF)


def layer_kernel(
    devices,
    tokens_h, norm_gain_h, decay_base_h, rate_base_h, head_gain_h, second_gain_h, ids_h, shares_h,
    unpack_h, pack_h, state, w_recept, w_keys, w_values, d_first, d_second, r_first, r_second, w_output,
    gate_h, up_h, down_h,
    st, ret_out, after_ref, blend_ref,
    tokens, norm_gain, decay_base, rate_base, head_gain, second_gain, ids, shares, unpack_m, pack_m,
    wr, wk, wv, df, ds, rf, rs, wo, gate, up, down,
    far_tokens, table, rowbuf, dh, w2, turned, v_turned, pq, pv, mixed_ref,
    tok_send, tok_buf, mix_send, mix_buf, own_rows, rows_x, hidden,
    part_f, part_b, peer_b, zsend, ret,
    s_sem, w_sem, in_sem, gsend, grecv, tsend, trecv, msend, mrecv, xsend, xrecv, ysend, yrecv, rsend, rrecv,
):
    heads, count, width, _ = st.shape
    model = tokens.shape[1]
    inner_mix = heads * width
    group = devices // EXPERTS
    me = lax.axis_index("ep")
    mine = lax.div(me, group)
    place = lax.rem(me, group)
    packed_rows = EXPERTS * ROWS
    rows = EXPERTS * CAP_DEV

    wide = inner_mix // MIX_CHUNKS
    half = heads // MIX_CHUNKS

    def load(i, src, dst):
        return pltpu.make_async_copy(src, dst, w_sem.at[i])

    def load_columns(i, n, src, dst):
        cols = pl.ds(n * wide, wide)
        return load(i, src.at[:, cols], dst.at[:, cols])

    low_loads = [
        load(i, src, dst)
        for i, (src, dst) in enumerate([(d_first, df), (r_first, rf), (d_second, ds), (r_second, rs)])
    ]
    mix_loads = [
        [
            load_columns(4 + 3 * n + i, n, src, dst)
            for i, (src, dst) in enumerate([(w_keys, wk), (w_values, wv), (w_recept, wr)])
        ]
        for n in range(MIX_CHUNKS)
    ]
    late = 4 + 3 * MIX_CHUNKS
    out_load, gate_load, up_load, down_load = [
        load(late + i, src, dst)
        for i, (src, dst) in enumerate([(w_output, wo), (gate_h, gate), (up_h, up), (down_h, down)])
    ]
    small_of = [
        (ids_h, ids), (shares_h, shares), (tokens_h, tokens), (norm_gain_h, norm_gain),
        (decay_base_h, decay_base), (rate_base_h, rate_base), (head_gain_h, head_gain),
        (second_gain_h, second_gain), (unpack_h, unpack_m), (pack_h, pack_m),
    ]
    smalls = [
        pltpu.make_async_copy(src, dst, s_sem.at[i]) for i, (src, dst) in enumerate(small_of)
    ]
    for copy in smalls:
        copy.start()
    for copy in low_loads + mix_loads[0]:
        copy.start()
    def fetch(h):
        return pltpu.make_async_copy(state.at[:, h], st.at[h], in_sem.at[h])

    def start_fetches(low, high):
        def step(h, c):
            fetch(h).start()
            return c

        lax.fori_loop(low, high, step, 0)

    start_fetches(0, half)
    for copy in mix_loads[1]:
        copy.start()
    start_fetches(half, heads)


    def other(i):
        total = 0
        for k in range(EXPERTS.bit_length() - 1):
            a = lax.rem(lax.div(mine, 1 << k), 2)
            b = lax.rem(lax.div(i, 1 << k), 2)
            total = total + (a + b - 2 * a * b) * (1 << k)
        return total

    others = [other(i) for i in range(EXPERTS - 1, 0, -1)]

    def each_other(body):
        for e in others:
            body(e)

    def peer(i):
        return lax.rem(place + i, group)

    barrier = pltpu.get_barrier_semaphore()

    def greet(e):
        pl.semaphore_signal(barrier, inc=1, device_id=(e * group + place,), device_id_type=MESH)

    each_other(greet)
    for i in range(1, group):
        pl.semaphore_signal(
            barrier, inc=1, device_id=(mine * group + peer(i),), device_id_type=MESH
        )

    for i in (0, 1, 2):
        smalls[i].wait()
    total_rows = ids.shape[1]
    spot = lax.broadcasted_iota(jnp.int32, (total_rows, count), 0)
    column = lax.broadcasted_iota(jnp.int32, (total_rows, count), 1)
    all_ids = ids[...].astype(F32).astype(BF)
    choose = jnp.where(spot == column + me * count, 1.0, 0.0).astype(BF)
    share_high, share_low = split(shares[...])
    my_shares = dot(share_high, choose) + dot(share_low, choose)
    expert_at = lax.broadcasted_iota(jnp.int32, (EXPERTS, count), 0).astype(F32)
    earlier = jnp.where(
        lax.broadcasted_iota(jnp.int32, (count, count), 0)
        < lax.broadcasted_iota(jnp.int32, (count, count), 1),
        1.0, 0.0,
    ).astype(BF)
    shape = (EXPERTS, ROWS, count)
    at = lax.broadcasted_iota(jnp.int32, shape, 1).astype(F32)

    def slots(chosen):
        ids_of = dot(all_ids, chosen)
        hits = [
            jnp.where(expert_at == ids_of[i:i + 1], 1.0, 0.0) for i in range(ids.shape[0])
        ]
        member = functools.reduce(jnp.add, hits)
        order = jnp.where(member > 0.5, dot(member.astype(BF), earlier), -1.0)
        slot = jnp.broadcast_to(order[:, None, :], shape)
        found = [
            (slot == (at - CAP_DEV) * PARTS + j) & (at >= CAP_DEV) for j in range(PARTS)
        ] + [(slot == at) & (at < CAP_DEV)]
        return hits, [jnp.where(f, 1.0, 0.0) for f in found]

    hits, found = slots(choose)
    share = functools.reduce(
        jnp.add, [hit * my_shares[i:i + 1] for i, hit in enumerate(hits)]
    )
    weight = jnp.broadcast_to(share[:, None, :], shape)
    for j in range(PARTS + 1):
        blend_ref[j] = (found[j] * weight).reshape(packed_rows, count)
        table[0, j] = found[j].reshape(packed_rows, count).astype(BF)

    def pack(which, values, put):
        part = values.shape[1] // (PARTS + 1)
        last = values[:, PARTS * part:]
        for j in range(PARTS):
            value = dot(table[which, PARTS], values[:, j * part:(j + 1) * part])
            value = value + dot(table[which, j], last)
            put(slice(j * part, (j + 1) * part), value.reshape(EXPERTS, ROWS, part).astype(BF))

    def put_tokens(which):
        def put(cols, value):
            tok_send[which, :, :, cols] = value

        return put

    far = other(EXPERTS // 2)
    far_device = far * group + place
    near = others[EXPERTS // 2:]

    def give_whole():
        return pltpu.make_async_remote_copy(
            src_ref=tokens, dst_ref=far_tokens, send_sem=gsend, recv_sem=grecv,
            device_id=(far_device,), device_id_type=MESH,
        )

    def give_tokens(which, e):
        return pltpu.make_async_remote_copy(
            src_ref=tok_send.at[which, e], dst_ref=tok_buf.at[far if which else mine],
            send_sem=tsend, recv_sem=trecv,
            device_id=(e * group + place,), device_id_type=MESH,
        )

    rest = pl.ds(0, EXPERTS - 1)

    def all_tokens():
        some = pl.ds(0, EXPERTS - 2)
        return pltpu.make_async_remote_copy(
            src_ref=tok_buf.at[some], dst_ref=tok_buf.at[some],
            send_sem=tsend, recv_sem=trecv,
            device_id=(others[0] * group + place,), device_id_type=MESH,
        )

    pl.semaphore_wait(barrier, EXPERTS - 1 + group - 1)
    give_whole().start()
    pack(0, tokens[...], put_tokens(0))
    for e in near:
        give_tokens(0, e).start()
    tok_buf[mine] = tok_send[0, mine]

    _, found = slots(jnp.where(spot == column + far_device * count, 1.0, 0.0).astype(BF))
    for j in range(PARTS + 1):
        table[1, j] = found[j].reshape(packed_rows, count).astype(BF)

    for i in range(3, len(smalls)):
        smalls[i].wait()
    resid = tokens[...].astype(F32)
    mean_sq = jnp.mean(resid * resid, axis=-1, keepdims=True)
    normed = (resid * lax.rsqrt(mean_sq + 1e-06) * norm_gain[...]).astype(BF)
    low_loads[0].wait()
    decay_low = jnp.tanh(dot(normed, df[...])).astype(BF)
    low_loads[1].wait()
    rate_low = dot(normed, rf[...]).astype(BF)
    low_loads[2].wait()
    low_loads[3].wait()

    same_head = (
        lax.broadcasted_iota(jnp.int32, (LANES, LANES), 0) // width
        == lax.broadcasted_iota(jnp.int32, (LANES, LANES), 1) // width
    )

    def head_sums(values, scale):
        ones = jnp.where(same_head, scale, 0.0).astype(BF)
        high, low = split(values)
        tiles = [slice(t, t + LANES) for t in range(0, values.shape[1], LANES)]
        return jnp.concatenate([dot(high[:, t], ones) + dot(low[:, t], ones) for t in tiles], axis=1)

    gap = jnp.zeros((STRIDE - count, wide), F32)

    side = lax.broadcasted_iota(jnp.int32, (wide, LANES), 1) // width
    own_side = lax.rem(lax.broadcasted_iota(jnp.int32, (wide, LANES), 0) // width, 2) == side

    def project(n):
        cols = slice(n * wide, (n + 1) * wide)
        pre = decay_base[:, cols] + dot(decay_low, ds[:, cols])
        d = jnp.exp(-jax.nn.sigmoid(pre) * math.exp(-0.5))
        a = jax.nn.sigmoid(rate_base[:, cols] + dot(rate_low, rs[:, cols]))
        if n == 0:
            mix_loads[0][0].wait()
        k = dot(normed, wk[:, cols]).astype(BF).astype(F32)
        if n == 0:
            mix_loads[0][1].wait()
        v = dot(normed, wv[:, cols]).astype(BF).astype(F32)
        if n == 0:
            mix_loads[0][2].wait()
        r = dot(normed, wr[:, cols]).astype(BF).astype(F32)
        sums = head_sums(jnp.concatenate([k * k, k * a * r, k * r], axis=0), 1.0)
        scale = lax.rsqrt(sums[:count] + 1e-06)
        unit = k * scale
        toward = d * r - unit * (sums[count:2 * count] * scale)
        rowbuf[0, :, cols] = d
        rowbuf[1, :, cols] = -unit * a
        rowbuf[2, :, cols] = k
        rowbuf[3, :, cols] = v * sums[2 * count:]
        tall = jnp.concatenate([unit, gap, toward, gap] * 2, axis=0)
        turned[cols, :] = jnp.where(own_side, tall.T, 0.0).astype(BF)
        tall = jnp.concatenate([jnp.zeros((STRIDE, wide), F32), v, gap] * 2, axis=0)
        v_turned[cols, :] = jnp.where(own_side, tall.T, 0.0)

    block = math.gcd(count, 8)
    lane = lax.broadcasted_iota(jnp.int32, (width, LANES), 1)
    lane_of = lax.rem(lane, STRIDE)

    def pairs(body, low, high):
        def step(t, c):
            for i in range(PAIRS_AT_ONCE):
                body(t * PAIRS_AT_ONCE + i)
            return c

        lax.fori_loop(low // PAIRS_AT_ONCE, high // PAIRS_AT_ONCE, step, 0)

    def first_pass(p):
        for i in range(2):
            fetch(2 * p + i).wait()
        span = pl.ds(pl.multiple_of(2 * p * width, 2 * width), 2 * width)
        right = turned[span, :]
        acc = jnp.zeros((width, LANES), F32)
        for g in range(count // block):
            some = [
                st[2 * p + i, g * block:(g + 1) * block].reshape(block * width, width).astype(BF)
                for i in range(2)
            ]
            got = dot(jnp.concatenate(some, axis=1), right).reshape(block, width, LANES)
            for i in range(block):
                acc = jnp.where(lane_of == g * block + i, got[i], acc)
        v_both = v_turned[span, :]
        v_both = v_both[:width] + v_both[width:]
        span = pl.ds(pl.multiple_of(p * width, width), width)
        pq[span, :] = acc
        pv[span, :] = jnp.where(lax.rem(lane, 2 * STRIDE) < STRIDE, acc, v_both)

    def give_mixed(n, e):
        return pltpu.make_async_remote_copy(
            src_ref=mix_send.at[n, e], dst_ref=mix_buf.at[n, mine],
            send_sem=msend.at[n], recv_sem=mrecv.at[n],
            device_id=(e * group + place,), device_id_type=MESH,
        )

    def all_mixed(n):
        return pltpu.make_async_remote_copy(
            src_ref=mix_send.at[n, rest], dst_ref=mix_buf.at[n, rest],
            send_sem=msend.at[n], recv_sem=mrecv.at[n],
            device_id=(others[0] * group + place,), device_id_type=MESH,
        )

    def mix_chunk(n):
        cols = slice(n * wide, (n + 1) * wide)
        both = pq[n * wide // 2:(n + 1) * wide // 2, :].T
        even, odd = both[STRIDE:STRIDE + count], both[3 * STRIDE:3 * STRIDE + count]
        low = lax.broadcasted_iota(jnp.int32, (count, LANES), 1) < width
        tiles = []
        for t in range(0, wide // 2, LANES):
            e, o = even[:, t:t + LANES], odd[:, t:t + LANES]
            tiles.append(jnp.where(low, e, pltpu.roll(o, width, axis=1)))
            tiles.append(jnp.where(low, pltpu.roll(e, width, axis=1), o))
        mixed = jnp.concatenate(tiles, axis=1) + rowbuf[3, :, cols]
        centre = mixed - head_sums(mixed, 1.0 / width)
        var = head_sums(centre * centre, 1.0 / width)
        out = (centre * lax.rsqrt(var + 0.00064) * head_gain[:, cols]).astype(BF)
        mixed_ref[:, cols] = out

        def put(at_cols, value):
            mix_send[n, :, :, at_cols] = value

        pack(0, out, put)
        mix_buf[n, mine] = mix_send[n, mine]

    def send_chunk(n):
        each_other(lambda e: give_mixed(n, e).start())

    batch = rows // 2
    my_half = lax.div(mine, EXPERTS // 2)
    halves = [1 - my_half, my_half]
    spans = [pl.ds(pl.multiple_of(h * batch, 16), batch) for h in halves]
    blocks = [pl.ds(h * (EXPERTS // 2), EXPERTS // 2) for h in halves]

    def unpack(source, width_of):
        part = width_of // (PARTS + 1)
        pieces, tail = [], jnp.zeros((batch, part), F32)
        for j in range(PARTS):
            value = source(slice(j * part, (j + 1) * part))
            value = value.astype(F32).reshape(packed_rows // 2, part).astype(BF)
            pieces.append(dot(unpack_m[PARTS], value))
            tail = tail + dot(unpack_m[j], value)
        return pieces + [tail]

    project(0)
    pairs(first_pass, 0, half // 2)
    for copy in mix_loads[1]:
        copy.wait()
    mix_chunk(0)
    project(1)
    send_chunk(0)
    give_whole().wait_recv()
    pack(1, far_tokens[...], put_tokens(1))
    tok_buf[far] = tok_send[1, mine]
    for e in near:
        give_tokens(1, e).start()
    pairs(first_pass, half // 2, half // 2 + half // 4)
    out_load.start()
    gate_load.start()
    pairs(first_pass, half // 2 + half // 4, half)
    mix_chunk(1)
    send_chunk(1)
    up_load.start()
    down_load.start()

    for h in range(heads):
        cols = slice(h * width, (h + 1) * width)
        dh[h] = rowbuf[0, :, cols]
        lines = [
            rowbuf[1, :, cols], jnp.zeros((STRIDE - count, width), F32),
            rowbuf[2, :, cols], jnp.zeros((STRIDE - count, width), F32),
        ]
        blank = [jnp.zeros((2 * STRIDE, width), F32)]
        lines = lines + blank if h % 2 == 0 else blank + lines
        w2[h] = jnp.concatenate(lines, axis=0).astype(BF)

    def second_pass(p):
        left = pv[pl.ds(pl.multiple_of(p * width, width), width), :]
        for g in range(count // block):
            some = range(g * block, (g + 1) * block)
            masked = jnp.concatenate([jnp.where(lane_of == b, left, 0.0) for b in some], axis=0)
            masked = masked.astype(BF)
            for i in range(2):
                h = 2 * p + i
                decay = dh[h]
                change = dot(masked, w2[h]).reshape(block, width, width)
                by = jnp.stack([jnp.broadcast_to(decay[b:b + 1], (width, width)) for b in some])
                st[h, g * block:(g + 1) * block] = st[h, g * block:(g + 1) * block] * by + change

    first_pairs = BESIDE[0] * heads // 32
    next_pairs = first_pairs + BESIDE[1] * heads // 32
    pairs(second_pass, 0, first_pairs)
    all_tokens().wait_recv()
    for b in range(2):
        for j, piece in enumerate(unpack(lambda cols: tok_buf[blocks[b], :, cols], model)):
            part = model // (PARTS + 1)
            own_rows[spans[b], j * part:(j + 1) * part] = piece
    out_load.wait()
    step_out = math.gcd(model, 256)

    def add_mixed(n, b):
        pieces = unpack(lambda cols: mix_buf[n, blocks[b], :, cols], wide)
        got = jnp.concatenate(pieces, axis=1).astype(BF)
        for t in range(model // step_out):
            cols = slice(t * step_out, (t + 1) * step_out)
            more = dot(got, wo[n * wide:(n + 1) * wide, cols])
            own_rows[spans[b], cols] = own_rows[spans[b], cols] + more

    for n in range(MIX_CHUNKS - 1):
        all_mixed(n).wait_recv()
        for b in range(2):
            add_mixed(n, b)
    all_mixed(MIX_CHUNKS - 1).wait_recv()

    def second_norm(values):
        mean_of = jnp.mean(values * values, axis=-1, keepdims=True)
        return (values * lax.rsqrt(mean_of + 1e-06) * second_gain[...]).astype(BF)

    def share_rows(b, i):
        return pltpu.make_async_remote_copy(
            src_ref=rows_x.at[place, spans[b]], dst_ref=rows_x.at[place, spans[b]],
            send_sem=xsend.at[b, peer(i)], recv_sem=xrecv.at[b, place],
            device_id=(mine * group + peer(i),), device_id_type=MESH,
        )

    def shared_rows(b, i):
        return pltpu.make_async_remote_copy(
            src_ref=rows_x.at[peer(i), spans[b]], dst_ref=rows_x.at[peer(i), spans[b]],
            send_sem=xsend.at[b, peer(i)], recv_sem=xrecv.at[b, peer(i)],
            device_id=(mine * group + peer(i),), device_id_type=MESH,
        )

    for b in range(2):
        add_mixed(MIX_CHUNKS - 1, b)
        rows_x[place, spans[b]] = second_norm(own_rows[spans[b], :])
        for i in range(1, group):
            share_rows(b, i).start()
    pairs(second_pass, first_pairs, next_pairs)
    gate_load.wait()
    up_load.wait()

    inner = gate.shape[1]
    step_in = math.gcd(inner, 256)

    chunk = model // OUT_CHUNKS
    small = math.gcd(chunk, 256)
    part = chunk // (PARTS + 1)
    low_mine = lax.rem(mine, EXPERTS // 2)
    targets = [
        [halves[0] * (EXPERTS // 2) + i for i in range(EXPERTS // 2)],
        [
            my_half * (EXPERTS // 2) + i + jnp.where(low_mine <= i, 1, 0)
            for i in range(EXPERTS // 2 - 1)
        ],
    ]

    def expand(b, low, high):
        left = jnp.concatenate([rows_x[q, spans[b], :] for q in range(group)], axis=0)
        for t in range(low, high):
            cols = slice(t * step_in, (t + 1) * step_in)
            g = dot(left, gate[:, cols])
            u = dot(left, up[:, cols])
            hidden[:, cols] = (g * jax.nn.sigmoid(g) * u).astype(BF)

    def swap(b, n, i):
        q = peer(i)
        return pltpu.make_async_remote_copy(
            src_ref=part_b.at[n, q, spans[b]], dst_ref=peer_b.at[n, place, spans[b]],
            send_sem=ysend.at[b, n, q], recv_sem=yrecv.at[b, n, place],
            device_id=(mine * group + q,), device_id_type=MESH,
        )

    def swapped(b, n, i):
        q = peer(i)
        return pltpu.make_async_remote_copy(
            src_ref=part_b.at[n, q, spans[b]], dst_ref=peer_b.at[n, q, spans[b]],
            send_sem=ysend.at[b, n, q], recv_sem=yrecv.at[b, n, q],
            device_id=(mine * group + q,), device_id_type=MESH,
        )

    def down_chunk(b, n):
        for t in range(chunk // small):
            cols = slice(n * chunk + t * small, n * chunk + (t + 1) * small)
            y = dot(hidden[...], down[:, cols])
            for q in range(group):
                piece = y[q * batch:(q + 1) * batch]
                part_f[n, q, spans[b], t * small:(t + 1) * small] = piece
                part_b[n, q, spans[b], t * small:(t + 1) * small] = piece.astype(BF)
        for i in range(1, group):
            swap(b, n, i).start()

    def give(n, e):
        return pltpu.make_async_remote_copy(
            src_ref=zsend.at[n, e], dst_ref=ret.at[n, mine],
            send_sem=rsend.at[n], recv_sem=rrecv.at[n],
            device_id=(e * group + place,), device_id_type=MESH,
        )

    def all_given(n):
        return pltpu.make_async_remote_copy(
            src_ref=zsend.at[n, rest], dst_ref=ret.at[n, rest],
            send_sem=rsend.at[n], recv_sem=rrecv.at[n],
            device_id=(others[0] * group + place,), device_id_type=MESH,
        )

    def return_chunk(b, n):
        for i in range(1, group):
            swapped(b, n, i).wait_recv()

        def summed(cols):
            total = part_f[n, place, spans[b], cols]
            for i in range(1, group):
                total = total + peer_b[n, peer(i), spans[b], cols].astype(F32)
            return total.astype(BF)

        last = summed(slice(PARTS * part, chunk))
        for j in range(PARTS):
            cols = slice(j * part, (j + 1) * part)
            value = dot(pack_m[PARTS], summed(cols)) + dot(pack_m[j], last)
            zsend[n, blocks[b], :, cols] = value.reshape(EXPERTS // 2, ROWS, part).astype(BF)
        for e in targets[b]:
            give(n, e).start()
        if b == 1:
            ret[n, mine] = zsend[n, mine]

    def rows_here(b):
        for i in range(1, group):
            shared_rows(b, i).wait_recv()

    steps = inner // step_in
    rows_here(0)
    expand(0, 0, steps)
    down_load.wait()
    for n in range(OUT_CHUNKS):
        down_chunk(0, n)
        if n >= LAG:
            return_chunk(0, n - LAG)
    rows_here(1)
    for n in range(OUT_CHUNKS - LAG, OUT_CHUNKS - 1):
        return_chunk(0, n)
    expand(1, 0, steps // 3)
    return_chunk(0, OUT_CHUNKS - 1)
    expand(1, steps // 3, steps)
    for n in range(OUT_CHUNKS):
        down_chunk(1, n)
        if n >= LAG:
            return_chunk(1, n - LAG)
    for n in range(OUT_CHUNKS - LAG, OUT_CHUNKS):
        return_chunk(1, n)

    pairs(second_pass, next_pairs, heads // 2)
    for t in range(model // step_out):
        cols = slice(t * step_out, (t + 1) * step_out)
        after_ref[:, cols] = tokens[:, cols].astype(F32) + dot(mixed_ref[...], wo[:, cols])

    give_whole().wait_send()
    all_tokens().wait_send()
    for n in range(MIX_CHUNKS):
        all_mixed(n).wait_send()
    for i in range(1, group):
        for b in range(2):
            share_rows(b, i).wait_send()
            for n in range(OUT_CHUNKS):
                swap(b, n, i).wait_send()
    for n in range(OUT_CHUNKS):
        all_given(n).wait_recv()
        ret_out[n] = ret[n]
    for n in range(OUT_CHUNKS):
        all_given(n).wait_send()


def finish_kernel(st, ret, after, blend_w, new_state, layer_out, out, sem, out_sem):
    heads = st.shape[0]

    def put(h):
        return pltpu.make_async_copy(st.at[h], new_state.at[:, h], sem.at[h])

    def start(h, c):
        put(h).start()
        return c

    lax.fori_loop(0, heads, start, 0)

    def dot_turned(left, right):
        return lax.dot_general(left, right, (((0,), (0,)), ((), ())), preferred_element_type=F32)

    high, low = split(blend_w[...])
    chunk = after.shape[1] // OUT_CHUNKS
    part = chunk // (PARTS + 1)
    packed_rows = EXPERTS * ROWS
    for n in range(OUT_CHUNKS):
        tail_at = slice(n * chunk + PARTS * part, (n + 1) * chunk)
        tail = after[:, tail_at]
        for j in range(PARTS):
            cols = slice(n * chunk + j * part, n * chunk + (j + 1) * part)
            block = ret[n, :, :, j * part:(j + 1) * part]
            block = block.astype(F32).reshape(packed_rows, part).astype(BF)
            value = after[:, cols] + dot_turned(high[PARTS], block) + dot_turned(low[PARTS], block)
            out[:, cols] = value.astype(BF)
            tail = tail + dot_turned(high[j], block) + dot_turned(low[j], block)
        out[:, tail_at] = tail.astype(BF)
    last = pltpu.make_async_copy(out, layer_out, out_sem.at[0])
    last.start()

    def end(h, c):
        put(h).wait()
        return c

    lax.fori_loop(0, heads, end, 0)
    last.wait()


def maps(experts):
    rows = experts * CAP_DEV
    row = np.arange(rows)[:, None]
    place = np.arange(experts * ROWS)[None, :]
    same = row // CAP_DEV == place // ROWS
    slot, at = row % CAP_DEV, place % ROWS
    found = [
        same & (at == CAP_DEV + slot // PARTS) & (slot % PARTS == j) for j in range(PARTS)
    ] + [same & (at == slot)]
    found = np.stack(found).astype(np.float32)
    return jnp.asarray(found, BF), jnp.asarray(found.transpose(0, 2, 1), BF)


def on_device(
    tokens, state, norm_gain, w_recept, w_keys, w_values, decay_base, decay_first_matrix,
    decay_second_matrix, rate_base, rate_first_matrix, rate_second_matrix, head_gain, w_output,
    second_gain, route_ids, route_weights, expert_gate, expert_up, expert_down,
):
    devices = lax.axis_size("ep")
    group = devices // EXPERTS
    count, heads, width, _ = state.shape
    model = tokens.shape[1]
    inner = expert_gate.shape[1]
    mix = heads * width
    rows = EXPERTS * CAP_DEV
    packed_rows = EXPERTS * ROWS
    folded = PARTS * model // (PARTS + 1)
    mix_fold = PARTS * (mix // MIX_CHUNKS) // (PARTS + 1)
    out_fold = PARTS * (model // OUT_CHUNKS) // (PARTS + 1)
    unpack_m, pack_m = maps(EXPERTS // 2)
    vm = pl.BlockSpec(memory_space=pltpu.VMEM)
    hb = pl.BlockSpec(memory_space=pl.ANY)
    dma = pltpu.SemaphoreType.DMA
    weights = [
        w_recept, w_keys, w_values, decay_first_matrix, decay_second_matrix, rate_first_matrix,
        rate_second_matrix, w_output, expert_gate, expert_up, expert_down,
    ]
    smalls = [
        tokens, norm_gain[None], decay_base[None], rate_base[None], head_gain[None],
        second_gain[None], route_ids.T, route_weights.T, unpack_m, pack_m,
    ]
    st, ret, after, blend_w = pl.pallas_call(
        functools.partial(layer_kernel, devices),
        out_shape=(
            pltpu.VMEM((heads, count, width, width), F32),
            pltpu.VMEM((OUT_CHUNKS, EXPERTS, ROWS, out_fold), BF),
            pltpu.VMEM((count, model), F32),
            pltpu.VMEM((PARTS + 1, packed_rows, count), F32),
        ),
        in_specs=[hb] * 22,
        out_specs=(vm, vm, vm, vm),
        scratch_shapes=[
            *[pltpu.VMEM(w.shape, w.dtype) for w in smalls],
            *[pltpu.VMEM(w.shape, BF) for w in weights],
            pltpu.VMEM((count, model), BF),
            pltpu.VMEM((2, PARTS + 1, packed_rows, count), BF),
            pltpu.VMEM((4, count, mix), F32),
            pltpu.VMEM((heads, count, width), F32),
            pltpu.VMEM((heads, LANES, width), BF),
            pltpu.VMEM((mix, LANES), BF),
            pltpu.VMEM((mix, LANES), F32),
            pltpu.VMEM((mix // 2, LANES), F32),
            pltpu.VMEM((mix // 2, LANES), F32),
            pltpu.VMEM((count, mix), BF),
            pltpu.VMEM((2, EXPERTS, ROWS, folded), BF),
            pltpu.VMEM((EXPERTS, ROWS, folded), BF),
            pltpu.VMEM((MIX_CHUNKS, EXPERTS, ROWS, mix_fold), BF),
            pltpu.VMEM((MIX_CHUNKS, EXPERTS, ROWS, mix_fold), BF),
            pltpu.VMEM((rows, model), F32),
            pltpu.VMEM((group, rows, model), BF),
            pltpu.VMEM((group * rows // 2, inner), BF),
            pltpu.VMEM((OUT_CHUNKS, group, rows, model // OUT_CHUNKS), F32),
            pltpu.VMEM((OUT_CHUNKS, group, rows, model // OUT_CHUNKS), BF),
            pltpu.VMEM((OUT_CHUNKS, group, rows, model // OUT_CHUNKS), BF),
            pltpu.VMEM((OUT_CHUNKS, EXPERTS, ROWS, out_fold), BF),
            pltpu.VMEM((OUT_CHUNKS, EXPERTS, ROWS, out_fold), BF),
            dma((len(smalls),)),
            dma((8 + 3 * MIX_CHUNKS,)),
            dma((heads,)),
            dma,
            dma,
            dma,
            dma,
            dma((MIX_CHUNKS,)),
            dma((MIX_CHUNKS,)),
            dma((2, group)),
            dma((2, group)),
            dma((2, OUT_CHUNKS, group)),
            dma((2, OUT_CHUNKS, group)),
            dma((OUT_CHUNKS,)),
            dma((OUT_CHUNKS,)),
        ],
        compiler_params=pltpu.CompilerParams(
            collective_id=0, has_side_effects=True, vmem_limit_bytes=49 * 1024 * 1024
        ),
        name="layer",
    )(
        *smalls, state, w_recept, w_keys, w_values, decay_first_matrix, decay_second_matrix, rate_first_matrix, rate_second_matrix,
        w_output, expert_gate, expert_up, expert_down,
    )
    new_state, layer_out = pl.pallas_call(
        finish_kernel,
        out_shape=(
            jax.ShapeDtypeStruct(state.shape, F32),
            jax.ShapeDtypeStruct((count, model), BF),
        ),
        in_specs=[vm] * 4,
        out_specs=(hb, hb),
        scratch_shapes=[pltpu.VMEM((count, model), BF), dma((heads,)), dma((1,))],
        compiler_params=pltpu.CompilerParams(vmem_limit_bytes=4 * 1024 * 1024),
        name="finish",
    )(st, ret, after, blend_w)
    return (layer_out, new_state)


def solution(mesh):
    rep = P()
    in_specs = (
        P("ep", None), P("ep", None, None, None), *[rep] * 15,
        P(None, "ep"), P(None, "ep"), P("ep", None),
    )
    out_specs = (P("ep", None), P("ep", None, None, None))
    return jax.shard_map(
        on_device, mesh=mesh, in_specs=in_specs, out_specs=out_specs, check_vma=False
    )
```

time: 54.7 us -> 45.2 us (0.83)
  Pallas kernels: 53.9 us -> 44.2 us
    pallas_call x1, Pallas kernels: 49.2 us -> 39.5 us  [on_device(): pl.pallas_call(functools.partial(layer_kernel, devices), out_shape=(pltpu...]
where the time goes in v2:
time: 45.2 us; the launch traced here: 45 us
  Pallas kernels  44.2 us (98%)
  between operations  0.81 us (2%)
    pallas_call x1, Pallas kernels, on_device(): pl.pallas_call(functools.partial(layer_kernel, devices), out_shape=(pltpu...  39.5 us
    pallas_call x1, Pallas kernels, on_device(): pl.pallas_call(finish_kernel, out_shape=(jax.ShapeDtypeStruct(state.shape...  4.72 us

profile of v2, /device:TPU:0, one launch (start us, length us, event | category | flops | bytes accessed | tf_op | source)
XLA Modules:
  0.0 45.0 jit_solution(7303350028610441523)
XLA Ops:
  0.6 39.5 %layer.1 = (f32[16,24,64,64]{3,2,1,0:T(8,128)S(1)}, bf16[4,16,8,384]{3,2,1,0:T(8,128)(2,1)S(1)}, f32[24,2048]{1,0:T(8,128)S(1)}, f32[4,128,24]{2,1,0:T(8,128)S(1)}) custom-call(bf16[24,2048]{1,0:T(8,128)(2,1)} %tokens_h.1, f32[1,2048]{1,0:T(1,128)} %bitcast.7, f32[1,1024]{1,0:T(1,128)} %bitcast.11, f32[1,1024]{1,0:T(1,128)} %bitcast.12, f32[1,1024]{1,0:T(1,128)} %bitcast.13, ...), custom_call_target="tpu_custom_call" | custom-call | tf_op jit(solution)/shard_map/layer/pallas_call | solution.py:685
  40.1 4.7 %finish.1 = (f32[24,16,64,64]{3,2,1,0:T(8,128)}, bf16[24,2048]{1,0:T(8,128)(2,1)}) custom-call(f32[16,24,64,64]{3,2,1,0:T(8,128)S(1)} %get-tuple-element.8.st, bf16[4,16,8,384]{3,2,1,0:T(8,128)(2,1)S(1)} %get-tuple-element.9.ret, f32[24,2048]{1,0:T(8,128)S(1)} %get-tuple-element.10.after, f32[4,128,24]{2,1,0:T(8,128)S(1)} %get-tuple-element.11.blend_w), custom_call_target="tpu_custom_call" | custom-call | tf_op jit(solution)/shard_map/finish/pallas_call | solution.py:744

commit v3 on v2

--- a/solution.py
+++ b/solution.py
@@ -19,6 +19,7 @@
 OUT_CHUNKS = 4
 PAIRS_AT_ONCE = 2
 LAG = 3
+URGENT = 1
 BESIDE = (8, 4)
 MESH = pl.DeviceIdType.MESH
 BF = jnp.bfloat16
@@ -56,6 +57,34 @@
     place = lax.rem(me, group)
     packed_rows = EXPERTS * ROWS
     rows = EXPERTS * CAP_DEV
+
+    def other(i):
+        total = 0
+        for k in range(EXPERTS.bit_length() - 1):
+            a = lax.rem(lax.div(mine, 1 << k), 2)
+            b = lax.rem(lax.div(i, 1 << k), 2)
+            total = total + (a + b - 2 * a * b) * (1 << k)
+        return total
+
+    others = [other(i) for i in range(EXPERTS - 1, 0, -1)]
+
+    def each_other(body):
+        for e in others:
+            body(e)
+
+    def peer(i):
+        return lax.rem(place + i, group)
+
+    barrier = pltpu.get_barrier_semaphore()
+
+    def greet(e):
+        pl.semaphore_signal(barrier, inc=1, device_id=(e * group + place,), device_id_type=MESH)
+
+    each_other(greet)
+    for i in range(1, group):
+        pl.semaphore_signal(
+            barrier, inc=1, device_id=(mine * group + peer(i),), device_id_type=MESH
+        )
 
     wide = inner_mix // MIX_CHUNKS
     half = heads // MIX_CHUNKS
@@ -111,34 +140,6 @@
     start_fetches(half, heads)
 
 
-    def other(i):
-        total = 0
-        for k in range(EXPERTS.bit_length() - 1):
-            a = lax.rem(lax.div(mine, 1 << k), 2)
-            b = lax.rem(lax.div(i, 1 << k), 2)
-            total = total + (a + b - 2 * a * b) * (1 << k)
-        return total
-
-    others = [other(i) for i in range(EXPERTS - 1, 0, -1)]
-
-    def each_other(body):
-        for e in others:
-            body(e)
-
-    def peer(i):
-        return lax.rem(place + i, group)
-
-    barrier = pltpu.get_barrier_semaphore()
-
-    def greet(e):
-        pl.semaphore_signal(barrier, inc=1, device_id=(e * group + place,), device_id_type=MESH)
-
-    each_other(greet)
-    for i in range(1, group):
-        pl.semaphore_signal(
-            barrier, inc=1, device_id=(mine * group + peer(i),), device_id_type=MESH
-        )
-
     for i in (0, 1, 2):
         smalls[i].wait()
     total_rows = ids.shape[1]
@@ -298,25 +299,48 @@
 
         lax.fori_loop(low // PAIRS_AT_ONCE, high // PAIRS_AT_ONCE, step, 0)
 
-    def first_pass(p):
-        for i in range(2):
-            fetch(2 * p + i).wait()
-        span = pl.ds(pl.multiple_of(2 * p * width, 2 * width), 2 * width)
-        right = turned[span, :]
-        acc = jnp.zeros((width, LANES), F32)
+    def first_pass(t):
+        low = t * PAIRS_AT_ONCE
+        for i in range(2 * PAIRS_AT_ONCE):
+            fetch(2 * low + i).wait()
+        spans_in = [
+            pl.ds(pl.multiple_of(2 * (low + i) * width, 2 * width), 2 * width)
+            for i in range(PAIRS_AT_ONCE)
+        ]
+        blank = jnp.zeros((2 * width, LANES), BF)
+        right = jnp.concatenate(
+            [
+                jnp.concatenate(
+                    [turned[at, :] if i == j else blank for j in range(PAIRS_AT_ONCE)], axis=1
+                )
+                for i, at in enumerate(spans_in)
+            ],
+            axis=0,
+        )
+        acc = [jnp.zeros((width, LANES), F32) for _ in range(PAIRS_AT_ONCE)]
         for g in range(count // block):
             some = [
-                st[2 * p + i, g * block:(g + 1) * block].reshape(block * width, width).astype(BF)
-                for i in range(2)
+                st[2 * low + i, g * block:(g + 1) * block].reshape(block * width, width).astype(BF)
+                for i in range(2 * PAIRS_AT_ONCE)
             ]
-            got = dot(jnp.concatenate(some, axis=1), right).reshape(block, width, LANES)
-            for i in range(block):
-                acc = jnp.where(lane_of == g * block + i, got[i], acc)
-        v_both = v_turned[span, :]
-        v_both = v_both[:width] + v_both[width:]
-        span = pl.ds(pl.multiple_of(p * width, width), width)
-        pq[span, :] = acc
-        pv[span, :] = jnp.where(lax.rem(lane, 2 * STRIDE) < STRIDE, acc, v_both)
+            got = dot(jnp.concatenate(some, axis=1), right)
+            for j in range(PAIRS_AT_ONCE):
+                here = got[:, j * LANES:(j + 1) * LANES].reshape(block, width, LANES)
+                for i in range(block):
+                    acc[j] = jnp.where(lane_of == g * block + i, here[i], acc[j])
+        for j in range(PAIRS_AT_ONCE):
+            v_both = v_turned[spans_in[j], :]
+            v_both = v_both[:width] + v_both[width:]
+            span = pl.ds(pl.multiple_of((low + j) * width, width), width)
+            pq[span, :] = acc[j]
+            pv[span, :] = jnp.where(lax.rem(lane, 2 * STRIDE) < STRIDE, acc[j], v_both)
+
+    def first_passes(low, high):
+        def step(t, c):
+            first_pass(t)
+            return c
+
+        lax.fori_loop(low // PAIRS_AT_ONCE, high // PAIRS_AT_ONCE, step, 0)
 
     def give_mixed(n, e):
         return pltpu.make_async_remote_copy(
@@ -374,7 +398,7 @@
         return pieces + [tail]
 
     project(0)
-    pairs(first_pass, 0, half // 2)
+    first_passes(0, half // 2)
     for copy in mix_loads[1]:
         copy.wait()
     mix_chunk(0)
@@ -385,10 +409,10 @@
     tok_buf[far] = tok_send[1, mine]
     for e in near:
         give_tokens(1, e).start()
-    pairs(first_pass, half // 2, half // 2 + half // 4)
+    first_passes(half // 2, half // 2 + half // 4)
     out_load.start()
     gate_load.start()
-    pairs(first_pass, half // 2 + half // 4, half)
+    first_passes(half // 2 + half // 4, half)
     mix_chunk(1)
     send_chunk(1)
     up_load.start()
@@ -421,11 +445,6 @@
     first_pairs = BESIDE[0] * heads // 32
     next_pairs = first_pairs + BESIDE[1] * heads // 32
     pairs(second_pass, 0, first_pairs)
-    all_tokens().wait_recv()
-    for b in range(2):
-        for j, piece in enumerate(unpack(lambda cols: tok_buf[blocks[b], :, cols], model)):
-            part = model // (PARTS + 1)
-            own_rows[spans[b], j * part:(j + 1) * part] = piece
     out_load.wait()
     step_out = math.gcd(model, 256)
 
@@ -435,12 +454,18 @@
         for t in range(model // step_out):
             cols = slice(t * step_out, (t + 1) * step_out)
             more = dot(got, wo[n * wide:(n + 1) * wide, cols])
-            own_rows[spans[b], cols] = own_rows[spans[b], cols] + more
+            own_rows[spans[b], cols] = more if n == 0 else own_rows[spans[b], cols] + more
 
     for n in range(MIX_CHUNKS - 1):
         all_mixed(n).wait_recv()
         for b in range(2):
             add_mixed(n, b)
+    all_tokens().wait_recv()
+    for b in range(2):
+        for j, piece in enumerate(unpack(lambda cols: tok_buf[blocks[b], :, cols], model)):
+            part = model // (PARTS + 1)
+            cols = slice(j * part, (j + 1) * part)
+            own_rows[spans[b], cols] = own_rows[spans[b], cols] + piece
     all_mixed(MIX_CHUNKS - 1).wait_recv()
 
     def second_norm(values):
@@ -549,10 +574,16 @@
             cols = slice(j * part, (j + 1) * part)
             value = dot(pack_m[PARTS], summed(cols)) + dot(pack_m[j], last)
             zsend[n, blocks[b], :, cols] = value.reshape(EXPERTS // 2, ROWS, part).astype(BF)
-        for e in targets[b]:
+        if b == 1:
+            for e in targets[1]:
+                give(n, e).start()
+            ret[n, mine] = zsend[n, mine]
+            return
+        for e in targets[0][:URGENT]:
             give(n, e).start()
-        if b == 1:
-            ret[n, mine] = zsend[n, mine]
+        for m in [n - 1] * (n > 0) + [n] * (n == OUT_CHUNKS - 1):
+            for e in targets[0][URGENT:]:
+                give(m, e).start()
 
     def rows_here(b):
         for i in range(1, group):

time: 45.2 us -> 44.4 us (0.982)
  Pallas kernels: 44.2 us -> 43.4 us
    pallas_call x1, Pallas kernels: 39.5 us -> 38.7 us  [on_device(): pl.pallas_call(functools.partial(layer_kernel, devices), out_shape=(pltpu...]
where the time goes in v3:
time: 44.4 us; the launch traced here: 44.2 us
  Pallas kernels  43.4 us (98%)
  between operations  0.81 us (2%)
    pallas_call x1, Pallas kernels, on_device(): pl.pallas_call(functools.partial(layer_kernel, devices), out_shape=(pltpu...  38.7 us
    pallas_call x1, Pallas kernels, on_device(): pl.pallas_call(finish_kernel, out_shape=(jax.ShapeDtypeStruct(state.shape...  4.72 us

profile of v3, /device:TPU:0, one launch (start us, length us, event | category | flops | bytes accessed | tf_op | source)
XLA Modules:
  0.0 44.2 jit_solution(11859016444350080712)
XLA Ops:
  0.6 38.7 %layer.1 = (f32[16,24,64,64]{3,2,1,0:T(8,128)S(1)}, bf16[4,16,8,384]{3,2,1,0:T(8,128)(2,1)S(1)}, f32[24,2048]{1,0:T(8,128)S(1)}, f32[4,128,24]{2,1,0:T(8,128)S(1)}) custom-call(bf16[24,2048]{1,0:T(8,128)(2,1)} %tokens_h.1, f32[1,2048]{1,0:T(1,128)} %bitcast.7, f32[1,1024]{1,0:T(1,128)} %bitcast.11, f32[1,1024]{1,0:T(1,128)} %bitcast.12, f32[1,1024]{1,0:T(1,128)} %bitcast.13, ...), custom_call_target="tpu_custom_call" | custom-call | tf_op jit(solution)/shard_map/layer/pallas_call | solution.py:716
  39.3 4.7 %finish.1 = (f32[24,16,64,64]{3,2,1,0:T(8,128)}, bf16[24,2048]{1,0:T(8,128)(2,1)}) custom-call(f32[16,24,64,64]{3,2,1,0:T(8,128)S(1)} %get-tuple-element.8.st, bf16[4,16,8,384]{3,2,1,0:T(8,128)(2,1)S(1)} %get-tuple-element.9.ret, f32[24,2048]{1,0:T(8,128)S(1)} %get-tuple-element.10.after, f32[4,128,24]{2,1,0:T(8,128)S(1)} %get-tuple-element.11.blend_w), custom_call_target="tpu_custom_call" | custom-call | tf_op jit(solution)/shard_map/finish/pallas_call | solution.py:775
